TPU v7x, 128 devices: a whole 4x4x4 slice. The times are simulated.
128 devices in a mesh: sp: 16 (over z, y), tp: 8 (over x, core).
Axes of the slice: x: 4, y: 4, z: 4, core: 2. Of those that a mesh axis runs over, the one named last changes fastest.
Arguments:
- layer_input: bfloat16 [16, 4096, 2048], P(None, ('sp', 'tp')), may hold values from -6 to 6
- input_gain: float32 [2048], replicated, may hold values from 0.5 to 1.5
- narrowing_matrix: bfloat16 [2048, 512], replicated, may hold values from -0.125 to 0.125
- rotary_down: bfloat16 [2048, 64], replicated, may hold values from -0.125 to 0.125
- summary_scaling: float32 [512], replicated, may hold values from 0.5 to 1.5
- lookup_widening: bfloat16 [512, 16, 128], P('tp'), may hold values from -0.25 to 0.25
- payload_widening: bfloat16 [512, 16, 128], P('tp'), may hold values from -0.25 to 0.25
- query_nope: bfloat16 [16, 16, 128], P('sp', 'tp'), may hold values from -6 to 6
- query_rotary: bfloat16 [16, 16, 64], P('sp', 'tp'), may hold values from -6 to 6
Outputs:
- stored_summaries: bfloat16 [16, 4096, 512], P('sp', None, 'tp')
- rotary_cache: bfloat16 [16, 4096, 64], P('sp', None, 'tp')
- first_read: bfloat16 [16, 16, 128], P('sp', 'tp')
All inputs are finite; a program needn't handle non-finite values.
Results may differ from a plain program's by a relative error of at most 0.02.
Values may be sent and summed in bfloat16 or wider, within the bound.
A program may use at most 64 MiB of HBM per device.

v0:
```python
import jax
import jax.numpy as jnp
from jax import lax
from jax.sharding import Mesh
from jax.sharding import PartitionSpec as P

QK_ROPE = 64
PLAIN_MATCH_SPAN = 128
TP = ("tp_0", "tp_1")
SP_TP = ("sp", "tp_0", "tp_1")


norm_eps = 1e-06
rotary_base = 10000.0


def joined_along(parts, dim):
    parts = jnp.moveaxis(parts, 0, dim)
    lengths = parts.shape
    return parts.reshape(*lengths[:dim], lengths[dim] * lengths[dim + 1], *lengths[dim + 2 :])


def gather_together(arrays, axis, dims):
    line = jnp.concatenate([a.reshape(-1) for a in arrays])
    lines, at, finished = lax.all_gather(line, axis), 0, []
    for a, dim in zip(arrays, dims):
        parts = lines[:, at : at + a.size].reshape(-1, *a.shape)
        finished.append(joined_along(parts, dim))
        at += a.size
    return tuple(finished)


def total_of_pieces(array, axis):
    parts = lax.all_gather(array, axis).astype(jnp.float32)
    return parts.sum(axis=0)


def summed_rows(term, width, axes):
    subtotal = term(jnp.int32(0), width * lax.axis_size(axes))
    for axis in axes:
        subtotal = lax.psum_scatter(subtotal, axis, scatter_dimension=0, tiled=True)
    return subtotal


def rescaled_lines(vector):
    return vector * lax.rsqrt(jnp.mean(vector * vector, axis=-1, keepdims=True) + norm_eps)


def rotate(vector, position):
    half_width = vector.shape[-1] // 2
    frequency = 1.0 / rotary_base ** (
        jnp.arange(half_width, dtype=jnp.float32) * 2.0 / vector.shape[-1]
    )
    angles = position * frequency
    first_half = vector[..., :half_width]
    second_half = vector[..., half_width:]
    return jnp.concatenate(
        [
            first_half * jnp.cos(angles) - second_half * jnp.sin(angles),
            second_half * jnp.cos(angles) + first_half * jnp.sin(angles),
        ],
        axis=-1,
    )


def to_pieces(array, sp_count, tp_count):
    seq_count, pos_local, cache_width = array.shape
    seq_each = seq_count // sp_count
    width_each = cache_width // tp_count
    array = array.reshape(sp_count, seq_each, pos_local, tp_count, width_each)
    array = array.transpose(0, 3, 1, 2, 4)
    return array.reshape(sp_count * tp_count, seq_each, pos_local, width_each)


def shards(
    layer_input,
    input_gain,
    narrowing_matrix,
    rotary_down,
    summary_scaling,
    lookup_widening,
    payload_widening,
    query_nope,
    query_rotary,
):
    seq_count, pos_local, feature_width = layer_input.shape
    sp_count = lax.axis_size("sp")
    tp_count = lax.axis_size(TP)
    block_index = lax.axis_index(SP_TP)
    normed = (rescaled_lines(layer_input.astype(jnp.float32)) * input_gain).astype(jnp.bfloat16)
    flat_rows = normed.reshape(seq_count * pos_local, feature_width)
    hidden_summary = jnp.dot(
        flat_rows, narrowing_matrix, preferred_element_type=jnp.float32
    ).astype(jnp.bfloat16)
    rotary = jnp.dot(flat_rows, rotary_down, preferred_element_type=jnp.float32).astype(
        jnp.bfloat16
    )
    hidden_summary = (
        (rescaled_lines(hidden_summary.astype(jnp.float32)) * summary_scaling)
        .astype(jnp.bfloat16)
        .reshape(seq_count, pos_local, -1)
    )
    positions = (block_index * pos_local + jnp.arange(pos_local, dtype=jnp.int32)).astype(
        jnp.float32
    )[None, :, None]
    rotary = rotate(rotary.astype(jnp.float32).reshape(seq_count, pos_local, -1), positions).astype(
        jnp.bfloat16
    )
    moved = (
        lax.all_to_all(
            to_pieces(hidden_summary, sp_count, tp_count),
            SP_TP,
            split_axis=0,
            concat_axis=2,
            tiled=True,
        ),
        lax.all_to_all(
            to_pieces(rotary, sp_count, tp_count), SP_TP, split_axis=0, concat_axis=2, tiled=True
        ),
    )
    hidden_summary = moved[0][0]
    rotary = moved[1][0]
    pos_total = hidden_summary.shape[1]
    rot_each = rotary.shape[2]
    head_each = query_nope.shape[1]
    query_all, turn_all = gather_together((query_nope, query_rotary), TP, (1, 1))
    absorbed = jnp.einsum(
        "shd,chd->shc", query_all, lookup_widening, preferred_element_type=jnp.float32
    ).astype(jnp.bfloat16)
    query_turned = rotate(turn_all.astype(jnp.float32), jnp.float32(pos_total)).astype(jnp.bfloat16)
    turned_mine = lax.dynamic_slice_in_dim(query_turned, lax.axis_index(TP) * rot_each, rot_each, 2)
    score_scale = (PLAIN_MATCH_SPAN + QK_ROPE) ** (-0.5)
    partial_value = (
        jnp.einsum("shc,spc->shp", absorbed, hidden_summary, preferred_element_type=jnp.float32)
        + jnp.einsum("shr,spr->shp", turned_mine, rotary, preferred_element_type=jnp.float32)
    ) * score_scale
    scores = total_of_pieces(partial_value.astype(jnp.bfloat16), TP).astype(jnp.float32)
    attention = jax.nn.softmax(scores, axis=-1).astype(jnp.bfloat16)
    context = jnp.einsum(
        "shp,spc->shc", attention, hidden_summary, preferred_element_type=jnp.float32
    ).astype(jnp.bfloat16)

    def project_heads(row_start, row_count):
        part_context = lax.dynamic_slice_in_dim(context, row_start, row_count, 1)
        part_weight = lax.dynamic_slice_in_dim(payload_widening, row_start, row_count, 1)
        return jnp.einsum(
            "shc,chv->hsv", part_context, part_weight, preferred_element_type=jnp.float32
        )

    values = summed_rows(project_heads, head_each, TP)
    first_read = rescaled_lines(values.transpose(1, 0, 2)).astype(jnp.bfloat16)
    return (hidden_summary, rotary, first_read)


def solution(mesh):
    torus = Mesh(mesh.devices.reshape(mesh.shape["sp"], 4, 2), ("sp", "tp_0", "tp_1"))
    in_specs = (
        P(None, SP_TP, None),
        P(),
        P(),
        P(),
        P(),
        P(TP, None, None),
        P(TP, None, None),
        P("sp", TP, None),
        P("sp", TP, None),
    )
    out_specs = (P("sp", None, TP), P("sp", None, TP), P("sp", TP, None))
    return jax.shard_map(
        shards, mesh=torus, in_specs=in_specs, out_specs=out_specs, check_vma=False
    )
```

profile of v0, /device:TPU:1, one launch (start us, length us, event | category | flops | bytes accessed | tf_op | source)
XLA Modules:
  0.0 117.1 jit_solution(14926533977251242927)
XLA Ops:
  7.2 2.2 %fusion.2 = f32[16,32]{1,0:T(8,128)S(1)} fusion(bf16[16,32,2048]{2,1,0:T(8,128)(2,1)} %param.9), kind=kLoop, calls=%fused_computation.5 | loop fusion | flops 3145216 | bytes 2099200 | tf_op jit(solution)/shard_map/reduce_sum | solution.py:46
  9.6 0.5 fusion.4
  10.1 1.3 %copy-done.2 = bf16[16,32,2048]{2,1,0:T(8,128)(2,1)} copy-done((bf16[16,32,2048]{2,1,0:T(8,128)(2,1)}, bf16[16,32,2048]{2,1,0:T(8,128)(2,1)S(1)}, u32[]{:S(2)}) %copy-start.2) | copy-done | bytes 2097176
  11.5 0.8 fusion.5
  13.0 0.8 reshape.408
  13.8 11.5 %all-to-all-start.1 = ((bf16[128,2,128]{2,1,0:T(2,128)(2,1)}), bf16[128,2,128]{2,1,0:T(2,128)(2,1)S(1)}, u32[]{:S(2)}, u32[]{:S(2)}) async-start(bf16[128,2,128]{2,1,0:T(2,128)(2,1)} %reshape.408), calls=%async_computation.1 | async-start | bytes 131072 | tf_op jit(solution)/shard_map/all_to_all | solution.py:117
  25.4 13.6 %all-gather.2 = bf16[8,1,384]{2,1,0:T(2,128)(2,1)S(1)} all-gather(bf16[1,1,384]{2,1,0:T(2,128)(2,1)S(1)} %reshape.390), channel_id=2, replica_groups=mesh['sp'=16,'tp_0'=4,'tp_1'=2] {'tp_0','tp_1'}, dimensions={0}, use_global_device_ids=true | all-gather | bytes 6912 | tf_op jit(solution)/shard_map/all_gather | solution.py:25
  39.0 2.9 %fusion.7 = (f32[512]{0:T(512)S(1)}, bf16[512,512]{0,1:T(8,128)(2,1)S(1)}) fusion(bf16[512,2048]{1,0:T(8,128)(2,1)} %bitcast.76, bf16[2048,512]{1,0:T(8,128)(2,1)S(1)} %copy-done), kind=kOutput, calls=%fused_computation.16 | convolution fusion | flops 1074789888 | bytes 4720640 | tf_op jit(solution)/shard_map/dot_general | solution.py:92
  42.2 1.0 copy.36
  43.2 1.6 %reshape_reshape.3 = bf16[16,1,32,8,64]{4,3,2,0,1:T(8,128)(2,1)S(1)} reshape(bf16[512,512]{1,0:T(8,128)(2,1)} %copy.36) | data formatting | bytes 1048576 | tf_op jit(solution)/shard_map/reshape;reshape | solution.py:70
  44.8 1.2 %copy.37 = bf16[16,8,1,32,64]{4,3,1,0,2:T(8,128)(2,1)} copy(bf16[16,8,1,32,64]{4,1,3,0,2:T(8,128)(2,1)S(1)} %bitcast.77) | data formatting | bytes 1048576 | tf_op jit(solution)/shard_map/transpose | solution.py:71
  46.0 3.0 %reshape.406 = bf16[128,2,1024]{2,1,0:T(2,128)(2,1)} reshape(bf16[128,1,32,64]{3,2,1,0:T(8,128)(2,1)} %bitcast.78) | data formatting | bytes 1048576
  49.1 9.0 %all-to-all-start = ((bf16[128,2,1024]{2,1,0:T(2,128)(2,1)}), bf16[128,2,1024]{2,1,0:T(2,128)(2,1)}, u32[]{:S(2)}, u32[]{:S(2)}) async-start(bf16[128,2,1024]{2,1,0:T(2,128)(2,1)} %reshape.406), calls=%async_computation | async-start | bytes 1048576 | tf_op jit(solution)/shard_map/all_to_all | solution.py:110
  58.3 0.2 fusion.15
  58.5 0.2 reshape.409
  58.8 0.3 reshape.382
  59.1 12.3 %all-to-all-done = bf16[128,2,1024]{2,1,0:T(2,128)(2,1)} async-done(((bf16[128,2,1024]{2,1,0:T(2,128)(2,1)}), bf16[128,2,1024]{2,1,0:T(2,128)(2,1)}, u32[]{:S(2)}, u32[]{:S(2)}) %all-to-all-start) | async-done | bytes 524320 | tf_op jit(solution)/shard_map/all_to_all | solution.py:110
  71.4 2.3 %reshape.407 = bf16[128,1,32,64]{3,2,1,0:T(8,128)(2,1)S(1)} reshape(bf16[128,2,1024]{2,1,0:T(2,128)(2,1)} %all-to-all-done) | data formatting | bytes 1048576
  73.6 0.4 fusion.26
  74.0 0.9 fusion.1
  74.9 0.6 dynamic-slice.2
  75.5 0.6 dynamic-slice
  77.4 0.9 squeeze.7
  78.3 1.1 copy.45
  79.5 15.4 %all-gather.5.cloned.1.call-done = bf16[128,4096]{1,0:T(8,128)(2,1)} async-done(((bf16[16,4096]{1,0:T(8,128)(2,1)}), bf16[128,4096]{1,0:T(8,128)(2,1)}) %all-gather.5.cloned.1.call-update) | async-done | bytes 1048592 | tf_op jit(solution)/shard_map/all_gather | solution.py:34
  94.9 1.4 %convert_reduce_fusion = f32[16,4096]{1,0:T(8,128)S(1)} fusion(bf16[8,16,4096]{2,1,0:T(8,128)(2,1)} %bitcast.80), kind=kLoop, calls=%fused_computation.8 | loop fusion | flops 983040 | bytes 1310720 | tf_op jit(solution)/shard_map/reduce_sum | solution.py:35
  96.4 0.2 exponential_reduce_fusion
  96.7 0.3 fusion.6
  97.0 1.1 fusion.13
  98.1 7.0 %all-reduce = f32[16,1,128]{2,0,1:T(8,128)S(1)} all-reduce(f32[16,1,128]{2,0,1:T(8,128)S(1)} %bitcast.86), channel_id=4, replica_groups=mesh['sp'=16,'tp_0'=4,'tp_1'=2] {'tp_0'}, use_global_device_ids=true, to_apply=%region_5.0.clone | all-reduce | flops 2048 | bytes 16384
  105.1 4.4 %all-reduce.1 = f32[4,1,128]{2,0,1:T(4,128)S(1)} all-reduce(f32[4,1,128]{2,0,1:T(4,128)S(1)} %constant_dynamic-slice_fusion), channel_id=5, replica_groups=mesh['sp'=16,'tp_0'=4,'tp_1'=2] {'tp_1'}, use_global_device_ids=true, to_apply=%region_6.0.clone | all-reduce | flops 512 | bytes 4096
  109.7 0.6 multiply_convert_fusion
  (49 shorter events, 1.7 us)
Async XLA Ops:
  7.2 31.8 %copy-start = (bf16[2048,512]{1,0:T(8,128)(2,1)S(1)}, bf16[2048,512]{1,0:T(8,128)(2,1)}, u32[]{:S(2)}) copy-start(bf16[2048,512]{1,0:T(8,128)(2,1)} %param.11) | copy-start | bytes 6291460
  7.2 2.3 %copy-start.4 = (f32[2048]{0:T(1024)S(1)}, f32[2048]{0:T(1024)}, u32[]{:S(2)}) copy-start(f32[2048]{0:T(1024)} %param.10) | copy-start | bytes 24580
  7.2 2.3 %copy-start.1 = (bf16[16,32,2048]{2,1,0:T(8,128)(2,1)S(1)}, bf16[16,32,2048]{2,1,0:T(8,128)(2,1)}, u32[]{:S(2)}) copy-start(bf16[16,32,2048]{2,1,0:T(8,128)(2,1)} %param.9) | copy-start | bytes 6291460
  9.6 1.9 %copy-start.3 = (bf16[2048,64]{0,1:T(8,128)(2,1)S(1)}, bf16[2048,64]{0,1:T(8,128)(2,1)}, u32[]{:S(2)}) copy-start(bf16[2048,64]{0,1:T(8,128)(2,1)} %param.12) | copy-start | bytes 786436
  10.1 1.4 %copy-start.2 = (bf16[16,32,2048]{2,1,0:T(8,128)(2,1)}, bf16[16,32,2048]{2,1,0:T(8,128)(2,1)S(1)}, u32[]{:S(2)}) copy-start(bf16[16,32,2048]{2,1,0:T(8,128)(2,1)S(1)} %fusion.4) | copy-start | bytes 6291460
  11.5 13.8 %copy-start.8 = (bf16[1,2,64]{2,1,0:T(2,128)(2,1)S(1)}, bf16[1,2,64]{2,1,0:T(2,128)(2,1)}, u32[]{:S(2)}) copy-start(bf16[1,2,64]{2,1,0:T(2,128)(2,1)} %param.17) | copy-start | bytes 772
  11.5 13.9 %copy-start.6 = (bf16[1,2,128]{2,1,0:T(2,128)(2,1)S(1)}, bf16[1,2,128]{2,1,0:T(2,128)(2,1)}, u32[]{:S(2)}) copy-start(bf16[1,2,128]{2,1,0:T(2,128)(2,1)} %param.16) | copy-start | bytes 1540
  13.8 35.3 %all-to-all-start.1 = ((bf16[128,2,128]{2,1,0:T(2,128)(2,1)}), bf16[128,2,128]{2,1,0:T(2,128)(2,1)S(1)}, u32[]{:S(2)}, u32[]{:S(2)}) async-start(bf16[128,2,128]{2,1,0:T(2,128)(2,1)} %reshape.408), calls=%async_computation.1 | async-start | bytes 131072 | tf_op jit(solution)/shard_map/all_to_all | solution.py:117
  39.0 2.9 %copy-start.5 = (f32[512]{0:T(512)S(1)}, f32[512]{0:T(512)}, u32[]{:S(2)}) copy-start(f32[512]{0:T(512)} %param.13) | copy-start | bytes 6148
  46.0 12.3 %copy-start.7 = (bf16[64,16,128]{2,1,0:T(8,128)(2,1)S(1)}, bf16[64,16,128]{2,1,0:T(8,128)(2,1)}, u32[]{:S(2)}) copy-start(bf16[64,16,128]{2,1,0:T(8,128)(2,1)} %param.14) | copy-start | bytes 786436
  49.1 22.3 %all-to-all-start = ((bf16[128,2,1024]{2,1,0:T(2,128)(2,1)}), bf16[128,2,1024]{2,1,0:T(2,128)(2,1)}, u32[]{:S(2)}, u32[]{:S(2)}) async-start(bf16[128,2,1024]{2,1,0:T(2,128)(2,1)} %reshape.406), calls=%async_computation | async-start | bytes 1048576 | tf_op jit(solution)/shard_map/all_to_all | solution.py:110
  58.1 36.8 %all-gather.5.cloned.1.call-start = ((), (), s32[]{:S(2)}) async-start(), calls=%async_computation.2 | async-start | bytes 1179648 | tf_op jit(solution)/shard_map/all_gather | solution.py:34
  58.7 16.2 %copy-start.10 = (u32[128]{0:T(128)S(1)}, u32[128]{0:T(128)}, u32[]{:S(2)}) copy-start(u32[128]{0:T(128)} %constant.62) | copy-start | bytes 1540
  58.7 16.8 %copy-start.9 = (u32[128]{0:T(128)S(1)}, u32[128]{0:T(128)}, u32[]{:S(2)}) copy-start(u32[128]{0:T(128)} %constant.58) | copy-start | bytes 1540
Sparse Core Ops, SparseCore 0:
  75.1 19.7 all-gather.4
where the time goes:
time: 118 us; the launch traced here: 117 us
  waiting for transfers between devices  27.8 us (24%)
  blocking collectives  25 us (21%)
  starting transfers between devices  20.6 us (17%)
  local copies, waits for them, and re-layouts  15.6 us (13%)
  between operations  15.6 us (13%)
  matrix products  6.64 us (6%)
  other arithmetic  5.98 us (5%)
    all_gather x1, waiting for transfers between devices, total_of_pieces(): parts = lax.all_gather(array, axis).astype(jnp.float32)  15.4 us
    all_gather x1, blocking collectives, gather_together(): lines, at, finished = (lax.all_gather(line, axis), 0, [])  13.6 us
    all_to_all x1, waiting for transfers between devices, shards(): lax.all_to_all(to_pieces(hidden_summary, sp_count, tp_count), SP_TP, spli...  12.3 us
    all_to_all x1, starting transfers between devices, shards(): lax.all_to_all(to_pieces(rotary, sp_count, tp_count), SP_TP, split_axis=0...  11.5 us
    unnamed x2, blocking collectives  11.4 us
    unnamed x32, local copies, waits for them, and re-layouts  10.1 us
    all_to_all x1, starting transfers between devices, shards(): lax.all_to_all(to_pieces(hidden_summary, sp_count, tp_count), SP_TP, spli...  9.02 us
    dot_general x1, matrix products, shards(): jnp.dot(flat_rows, narrowing_matrix, preferred_element_type=jnp.float32)  2.91 us
  transfers between devices with their start and end apart: 3, of which 2 were waited for; matrix products, arithmetic and copies ran while one was open for 12% of the time, Pallas kernels for 0%

commit v1 on v0

v1 whole, which is shorter than its diff:
```python
import jax
import jax.numpy as jnp
import numpy as np
from jax import lax
from jax.experimental import pallas as pl
from jax.experimental.pallas import tpu as pltpu
from jax.sharding import PartitionSpec as P

MESH = pl.DeviceIdType.MESH
EPS = 1e-6
ROPE_BASE = 10000.0
F32 = jnp.float32
BF16 = jnp.bfloat16

NT = (((1,), (1,)), ((), ()))


def trig_tables(blocks, rows, rope):
    half = rope // 2
    freq = 1.0 / ROPE_BASE ** (np.arange(half, dtype=np.float64) * 2.0 / rope)
    freq = np.concatenate([freq, freq])
    first = np.arange(blocks + 8, dtype=np.float64)[:, None] * rows * freq
    offset = np.arange(rows, dtype=np.float64)[:, None] * freq

    def both(angle):
        return np.concatenate([np.cos(angle), np.sin(angle)], axis=1).astype(np.float32)

    return both(first), both(offset)


def half_swap(v):
    half = v.shape[-1] // 2
    return jnp.concatenate([v[:, half:], v[:, :half]], axis=1)


def iota(shape, dim):
    return lax.broadcasted_iota(jnp.int32, shape, dim)


def kernel(
    x_hbm, gain_hbm, w_hbm, rd_hbm, scal_hbm, look_hbm, pay_hbm, qn_hbm, qr_hbm, tab_hbm, off_hbm,
    out_s, out_r, out_f,
    xb, gain, w, rd, scal, look, pay, tab, off,
    kst, kall, qn, qr, aall, pst, pall, ktst, rtst, krecv, rrecv, asc, arecv, sbuf,
    ostage, rstage, fstage,
    lsem, wsem, ksend, krsem, qsend, qrsem, asend, arsem, psend, prsem, k2send, k2rsem, csend, crsem, osem,
):
    sp, tp = lax.axis_index("sp"), lax.axis_index("tp")
    z, y = sp // 4, lax.rem(sp, 4)

    def sp_of(dz, dy):
        return lax.rem(z + dz, 4) * 4 + lax.rem(y + dy, 4)

    def tp_of(step):
        return lax.rem(tp + step, 8)

    def x_copy(n):
        return pltpu.make_async_copy(x_hbm.at[sp_of((n // 4 + 1) % 4, n % 4)], xb.at[n], lsem.at[n])

    loads = [
        pltpu.make_async_copy(src, dst, wsem.at[n])
        for n, (src, dst) in enumerate(
            (
                (gain_hbm, gain), (w_hbm, w), (rd_hbm, rd), (scal_hbm, scal), (tab_hbm, tab), (off_hbm, off),
                (look_hbm, look), (pay_hbm, pay), (qn_hbm, qn.at[tp]), (qr_hbm, qr.at[tp]),
            )
        )
    ]
    for n in range(4):
        x_copy(n).start()
    for c in loads[:6]:
        c.start()
    for n in range(4, 16):
        x_copy(n).start()
    for c in loads[6:]:
        c.start()

    barrier = pltpu.get_barrier_semaphore()

    def greet_sp(n, _):
        pl.semaphore_signal(barrier, inc=1, device_id=(lax.rem(sp + n, 16), tp), device_id_type=MESH)
        return 0

    def greet_tp(n, _):
        pl.semaphore_signal(barrier, inc=1, device_id=(sp, tp_of(n)), device_id_type=MESH)
        return 0

    lax.fori_loop(1, 16, greet_sp, 0)
    lax.fori_loop(1, 8, greet_tp, 0)

    def to_tp(src, dst, send, recv, step):
        return pltpu.make_async_remote_copy(
            src_ref=src, dst_ref=dst, send_sem=send, recv_sem=recv,
            device_id=(sp, tp_of(step)), device_id_type=MESH,
        )

    def q_copies(step, at):
        return (
            to_tp(qn_hbm, qn.at[at], qsend.at[0, step], qrsem.at[0, at], step),
            to_tp(qr_hbm, qr.at[at], qsend.at[1, step], qrsem.at[1, at], step),
        )

    def k_copy(n, dz, dy, slot):
        return pltpu.make_async_remote_copy(
            src_ref=kst.at[n], dst_ref=kall.at[slot], send_sem=ksend.at[n], recv_sem=krsem.at[slot],
            device_id=(sp_of(dz, dy), tp), device_id_type=MESH,
        )

    my_slot = 4 * z + lax.rem(y + tp, 4)

    for c in loads[:6]:
        c.wait()
    sign = jnp.where(iota((32, 64), 1) < 32, -1.0, 1.0).astype(F32)
    base = tab[pl.ds(sp * 8 + tp, 1), :]
    offs = off[...]
    cos = base[:, :64] * offs[:, :64] - base[:, 64:] * offs[:, 64:]
    sin = (base[:, 64:] * offs[:, :64] + base[:, :64] * offs[:, 64:]) * sign
    cos4 = jnp.concatenate([cos] * 4, axis=0)
    sin4 = jnp.concatenate([sin] * 4, axis=0)

    def project(k, _):
        dz = lax.rem(k + 1, 4)
        for dy in range(4):
            pltpu.make_async_copy(x_hbm.at[0], xb.at[4 * k + dy], lsem.at[4 * k + dy]).wait()
        xv = xb[pl.ds(4 * k, 4)].reshape(128, 2048).astype(F32)
        scale = lax.rsqrt(jnp.mean(xv * xv, axis=1, keepdims=True) + EPS)
        normed = (xv * scale * gain[...]).astype(BF16)
        latent = jnp.dot(normed, w[...], preferred_element_type=F32).astype(BF16).astype(F32)
        rot = lax.dot_general(normed, rd[...], NT, preferred_element_type=F32).astype(BF16).astype(F32)
        scale = lax.rsqrt(jnp.mean(latent * latent, axis=1, keepdims=True) + EPS)
        stored = (latent * scale * scal[...]).astype(BF16)
        turned = rot * cos4 + half_swap(rot) * sin4
        turned = jnp.concatenate([turned, jnp.zeros_like(turned)], axis=1).astype(BF16)
        kst[pl.ds(4 * k, 4), :, :512] = stored.reshape(4, 32, 512)
        kst[pl.ds(4 * k, 4), :, 512:] = turned.reshape(4, 32, 128)

        @pl.when(k == 3)
        def _():
            kall[my_slot, :, :512] = stored[:32]
            kall[my_slot, :, 512:] = turned[:32]

        @pl.when(k == 0)
        def _():
            pl.semaphore_wait(barrier, 22)

            def send_q(step, _):
                for c in q_copies(step, tp):
                    c.start()
                return 0

            lax.fori_loop(1, 8, send_q, 0)

        for dy in range(1, 4):
            k_copy(4 * k + dy, dz, dy, my_slot).start()

        @pl.when(k < 3)
        def _():
            k_copy(4 * k, dz, 0, my_slot).start()

        return 0

    lax.fori_loop(0, 4, project, 0)

    for c in loads[6:]:
        c.wait()

    def wait_q(step, _):
        for c in q_copies(step, tp_of(8 - step)):
            c.wait_recv()
        return 0

    lax.fori_loop(1, 8, wait_q, 0)
    q_all = qn[...].astype(F32).reshape(16, 128).astype(BF16)
    t_all = qr[...].astype(F32).reshape(16, 64)
    parts = lax.dot_general(q_all, look[...], NT, preferred_element_type=F32)
    same = jnp.bitwise_and(iota((16, 1024), 1), 15) == iota((16, 1024), 0)
    parts = jnp.where(same, parts, 0.0).astype(BF16)
    pick = jnp.right_shift(iota((1024, 128), 0), 4) + 64 * lax.rem(tp, 2) == iota((1024, 128), 1)
    pick = jnp.where(pick, 1.0, 0.0).astype(BF16)
    aall[tp] = jnp.dot(parts, pick, preferred_element_type=F32).astype(BF16)
    last = tab[128:129, :]
    q_turn = t_all * last[:, :64] + half_swap(t_all) * (last[:, 64:] * sign[:1])
    q_turn = jnp.concatenate([q_turn, jnp.zeros_like(q_turn)], axis=1).astype(BF16)

    def a_copy(step, at):
        return to_tp(aall.at[tp], aall.at[at], asend.at[step], arsem.at[at], step)

    def send_a(step, _):
        a_copy(step, tp).start()
        return 0

    lax.fori_loop(1, 8, send_a, 0)

    row, col = iota((256, 256), 0), iota((256, 256), 1)
    wanted = jnp.bitwise_and(row, 15) * 16 + jnp.right_shift(row, 4)
    order = jnp.where(col == wanted, 1.0, 0.0).astype(BF16)
    for g in range(4):
        rows = jnp.dot(order, pay[256 * g : 256 * (g + 1), :], preferred_element_type=F32)
        pst[:, :, 16 * g : 16 * (g + 1), :] = rows.astype(BF16).reshape(8, 2, 16, 128)
    pall[:, pl.ds(pl.multiple_of(tp * 64, 64), 64), :] = pst[tp]

    def p_copy(step, at):
        there = pall.at[:, pl.ds(pl.multiple_of(at * 64, 64), 64), :]
        return to_tp(pst.at[tp_of(step)], there, psend.at[step], prsem.at[at], step)

    def send_p(step, _):
        p_copy(step, tp).start()
        return 0

    lax.fori_loop(1, 8, send_p, 0)

    def wait_a(step, _):
        a_copy(step, tp_of(8 - step)).wait_recv()
        return 0

    lax.fori_loop(1, 8, wait_a, 0)
    absorbed = jnp.concatenate([aall[2 * u] + aall[2 * u + 1] for u in range(4)] + [q_turn], axis=1)

    def k2_copies(step, g, at):
        return (
            to_tp(ktst.at[g, tp_of(step)], krecv.at[g, at], k2send.at[0, g, step], k2rsem.at[0, g, at], step),
            to_tp(rtst.at[g, tp_of(step)], rrecv.at[g, at], k2send.at[1, g, step], k2rsem.at[1, g, at], step),
        )

    def group_of(k):
        return lax.rem(z + 3 - k, 4)

    def spread(k, _):
        g = group_of(k)
        for dy in range(1, 4):
            k_copy(4 * k + dy, 0, dy, 4 * g + lax.rem(y + 4 - dy + tp, 4)).wait_recv()

        @pl.when(k < 3)
        def _():
            k_copy(4 * k, 0, 1, 4 * g + lax.rem(y + tp, 4)).wait_recv()

        turned_over = kall[pl.ds(4 * g, 4)].reshape(128, 640).T
        ktst[g] = turned_over[:512].reshape(8, 64, 128)
        rtst[g] = turned_over[512:576].astype(F32).reshape(8, 8, 128).astype(BF16)

        def send(step, _):
            for c in k2_copies(step, g, tp):
                c.start()
            return 0

        lax.fori_loop(1, 8, send, 0)
        krecv[g, tp] = ktst[g, tp]
        rrecv[g, tp] = rtst[g, tp]
        sbuf[k] = jnp.dot(absorbed, turned_over, preferred_element_type=F32) * (192.0 ** -0.5)
        return 0

    lax.fori_loop(0, 4, spread, 0)

    scores = jnp.concatenate([sbuf[k] for k in range(4)], axis=1)
    top = jnp.max(scores, axis=1, keepdims=True)
    weight = jnp.exp(scores - top)
    total = jnp.sum(weight, axis=1, keepdims=True)
    context = jnp.zeros((16, 512), F32)
    for k in range(4):
        rows = kall[pl.ds(4 * group_of(k), 4), :, :512].reshape(128, 512)
        context += jnp.dot(
            weight[:, 128 * k : 128 * (k + 1)].astype(BF16), rows, preferred_element_type=F32
        )
    stats = jnp.where(iota((16, 128), 1) < 64, top, total)
    for t in range(8):
        asc[t, :, :512] = context[2 * t : 2 * t + 2]
        asc[t, :, 512:] = stats[2 * t : 2 * t + 2]

    def c_copy(step, at):
        return to_tp(asc.at[tp_of(step)], arecv.at[at], csend.at[step], crsem.at[at], step)

    def send_c(step, _):
        c_copy(step, tp).start()
        return 0

    lax.fori_loop(1, 8, send_c, 0)
    arecv[tp] = asc[tp]

    def wait_c(step, _):
        c_copy(step, tp_of(8 - step)).wait_recv()
        p_copy(step, tp_of(8 - step)).wait_recv()
        return 0

    lax.fori_loop(1, 8, wait_c, 0)
    got = arecv[...]
    tops, totals = got[:, :, 512:513], got[:, :, 576:577]
    share = jnp.exp(tops - jnp.max(tops, axis=0, keepdims=True))
    summed = jnp.sum(got[:, :, :512] * share, axis=0) / jnp.sum(totals * share, axis=0)
    mixed = jnp.concatenate([summed, jnp.zeros((14, 512), F32)], axis=0).astype(BF16)
    first = jnp.dot(mixed, pall[0], preferred_element_type=F32)
    second = jnp.dot(mixed, pall[1], preferred_element_type=F32)
    values = jnp.where(iota((16, 128), 0) == 0, first, second)[:2]
    values = values * lax.rsqrt(jnp.mean(values * values, axis=1, keepdims=True) + EPS)
    fstage[...] = values.astype(BF16)
    pltpu.make_async_copy(fstage, out_f, osem.at[8]).start()

    def out_copies(g):
        lanes = pl.ds(pl.multiple_of(g * 1024, 1024), 1024)
        return (
            pltpu.make_async_copy(ostage.at[g], out_s.at[:, lanes], osem.at[g]),
            pltpu.make_async_copy(rstage.at[g], out_r.at[:, lanes], osem.at[4 + g]),
        )

    def finish(k, _):
        g = group_of(k)

        def wait(step, _):
            for c in k2_copies(step, g, tp_of(8 - step)):
                c.wait_recv()
            return 0

        lax.fori_loop(1, 8, wait, 0)
        for source, stage, rows in ((krecv, ostage, 64), (rrecv, rstage, 8)):
            lane = jnp.right_shift(iota((rows, 128), 1), 5)
            for u in range(2):
                blocks = [source[g, 4 * u + j].astype(F32) for j in range(4)]
                for a in range(4):
                    mine = [jnp.bitwise_and(lane - a, 3) == j for j in range(3)]
                    v = jnp.where(
                        mine[0], blocks[0], jnp.where(mine[1], blocks[1], jnp.where(mine[2], blocks[2], blocks[3]))
                    )
                    if a:
                        v = pltpu.roll(v, 128 - 32 * a, 1)
                    at = 256 * a + 128 * u
                    stage[g, :, at : at + 128] = v.astype(BF16)
        for c in out_copies(g):
            c.start()
        return 0

    lax.fori_loop(0, 4, finish, 0)

    def drain(step, _):
        for c in q_copies(step, tp) + (a_copy(step, tp), p_copy(step, tp), c_copy(step, tp)):
            c.wait_send()
        for g in range(4):
            for c in k2_copies(step, g, tp):
                c.wait_send()
        return 0

    lax.fori_loop(1, 8, drain, 0)
    for n in range(16):
        if n != 12:
            k_copy(n, (n // 4 + 1) % 4, n % 4, my_slot).wait_send()
    for g in range(4):
        for c in out_copies(g):
            c.wait()
    pltpu.make_async_copy(fstage, out_f, osem.at[8]).wait()


def solution(mesh):
    first, offset = trig_tables(128, 32, 64)

    def step(x, gain, w, rd, scal, look, payload, qn, qr):
        any_space = pl.BlockSpec(memory_space=pl.ANY)
        dma = pltpu.SemaphoreType.DMA
        stored, rotary, read = pl.pallas_call(
            kernel,
            out_shape=(
                jax.ShapeDtypeStruct((64, 4096), BF16),
                jax.ShapeDtypeStruct((8, 4096), BF16),
                jax.ShapeDtypeStruct((2, 128), BF16),
            ),
            in_specs=[any_space] * 11,
            out_specs=(any_space,) * 3,
            scratch_shapes=[
                pltpu.VMEM((16, 32, 2048), BF16),
                pltpu.VMEM((1, 2048), F32),
                pltpu.VMEM((2048, 512), BF16),
                pltpu.VMEM((64, 2048), BF16),
                pltpu.VMEM((1, 512), F32),
                pltpu.VMEM((1024, 128), BF16),
                pltpu.VMEM((1024, 128), BF16),
                pltpu.VMEM((136, 128), F32),
                pltpu.VMEM((32, 128), F32),
                pltpu.VMEM((16, 32, 640), BF16),
                pltpu.VMEM((16, 32, 640), BF16),
                pltpu.VMEM((8, 2, 128), BF16),
                pltpu.VMEM((8, 2, 64), BF16),
                pltpu.VMEM((8, 16, 128), BF16),
                pltpu.VMEM((8, 2, 64, 128), BF16),
                pltpu.VMEM((2, 512, 128), BF16),
                pltpu.VMEM((4, 8, 64, 128), BF16),
                pltpu.VMEM((4, 8, 8, 128), BF16),
                pltpu.VMEM((4, 8, 64, 128), BF16),
                pltpu.VMEM((4, 8, 8, 128), BF16),
                pltpu.VMEM((8, 2, 640), F32),
                pltpu.VMEM((8, 2, 640), F32),
                pltpu.VMEM((4, 16, 128), F32),
                pltpu.VMEM((4, 64, 1024), BF16),
                pltpu.VMEM((4, 8, 1024), BF16),
                pltpu.VMEM((2, 128), BF16),
                dma((16,)),
                dma((10,)),
                dma((16,)),
                dma((16,)),
                dma((2, 8)),
                dma((2, 8)),
                dma((8,)),
                dma((8,)),
                dma((8,)),
                dma((8,)),
                dma((2, 4, 8)),
                dma((2, 4, 8)),
                dma((8,)),
                dma((8,)),
                dma((9,)),
            ],
            compiler_params=pltpu.CompilerParams(
                collective_id=0, has_side_effects=True, vmem_limit_bytes=48 * 1024 * 1024
            ),
        )(
            x, gain.reshape(1, 2048), w, rd.T, scal.reshape(1, 512), look.reshape(1024, 128),
            payload.reshape(1024, 128), qn.reshape(2, 128), qr.reshape(2, 64), jnp.asarray(first), jnp.asarray(offset),
        )
        return stored.T[None], rotary.T[None], read[None]

    tp = "tp"
    both = ("sp", "tp")
    in_specs = (
        P(None, both, None), P(), P(), P(), P(), P(tp, None, None), P(tp, None, None),
        P("sp", tp, None), P("sp", tp, None),
    )
    out_specs = (P("sp", None, tp), P("sp", None, tp), P("sp", tp, None))
    return jax.shard_map(step, mesh=mesh, in_specs=in_specs, out_specs=out_specs, check_vma=False)
```

time: 118 us -> 46.5 us (0.39)
  Pallas kernels: 0 us -> 33.1 us
  waiting for transfers between devices: 27.8 us -> 0 us
  blocking collectives: 25 us -> 0 us
  starting transfers between devices: 20.6 us -> 0 us
  between operations: 15.6 us -> 0.66 us
  matrix products: 6.64 us -> 0 us
  other arithmetic: 5.98 us -> 0 us
  local copies, waits for them, and re-layouts: 15.6 us -> 12.2 us
    pallas_call x0 -> x1, Pallas kernels: none -> 33.1 us  [step(): pl.pallas_call(kernel, out_shape=(jax.ShapeDtypeStruct((64, 4096), BF16),...]
    all_to_all x2 -> x0, starting transfers between devices: 20.5 us -> none  [the longest x1 11.5 us: shards(): lax.all_to_all(to_pieces(rotary, sp_count, tp_count), SP_TP, split_axis=0...]
    all_gather x1 -> x0, waiting for transfers between devices: 15.4 us -> none  [total_of_pieces(): parts = lax.all_gather(array, axis).astype(jnp.float32)]
    all_gather x1 -> x0, blocking collectives: 13.6 us -> none  [gather_together(): lines, at, finished = (lax.all_gather(line, axis), 0, [])]
    all_to_all x2 -> x0, waiting for transfers between devices: 12.3 us -> none  [the longest x1 12.3 us: shards(): lax.all_to_all(to_pieces(hidden_summary, sp_count, tp_count), SP_TP, spli...]
    unnamed x2 -> x0, blocking collectives: 11.4 us -> none
    dot_general x7 -> x0, matrix products: 6.64 us -> none  [the longest x1 2.91 us: shards(): jnp.dot(flat_rows, narrowing_matrix, preferred_element_type=jnp.float32)]
    reduce_sum x4 -> x0, other arithmetic: 3.97 us -> none  [the longest x2 2.34 us: rescaled_lines(): jnp.mean(vector * vector, axis=-1, keepdims=True) + norm_eps]
  transfers between devices with their start and end apart: 3 -> 0, of which waited for: 2 -> 0; matrix products, arithmetic and copies ran while one was open for 12% -> 0% of each run, Pallas kernels for 0% -> 0%
where the time goes in v1:
time: 46.5 us; the launch traced here: 46 us
  Pallas kernels  33.1 us (71%)
  local copies, waits for them, and re-layouts  12.2 us (26%)
  between operations  0.66 us (1%)
    pallas_call x1, Pallas kernels, step(): pl.pallas_call(kernel, out_shape=(jax.ShapeDtypeStruct((64, 4096), BF16),...  33.1 us
    unnamed x25, local copies, waits for them, and re-layouts  12.2 us

profile of v1, /device:TPU:1, one launch (start us, length us, event | category | flops | bytes accessed | tf_op | source)
XLA Modules:
  0.0 46.0 jit_solution(5320050250893128907)
XLA Ops:
  0.6 0.0 copy-start
  0.6 1.6 %copy-done = bf16[16,32,2048]{2,1,0:T(8,128)(2,1)S(1)} copy-done((bf16[16,32,2048]{2,1,0:T(8,128)(2,1)S(1)}, bf16[16,32,2048]{2,1,0:T(8,128)(2,1)}, u32[]{:S(2)}) %copy-start) | copy-done | bytes 2097176
  2.2 0.0 copy-start.1
  2.2 1.6 %copy-done.1 = bf16[2048,512]{1,0:T(8,128)(2,1)S(1)} copy-done((bf16[2048,512]{1,0:T(8,128)(2,1)S(1)}, bf16[2048,512]{1,0:T(8,128)(2,1)}, u32[]{:S(2)}) %copy-start.1) | copy-done | bytes 2097176
  3.8 0.0 copy-start.2
  3.8 0.9 %copy-done.2 = bf16[2048,64]{0,1:T(8,128)(2,1)S(1)} copy-done((bf16[2048,64]{0,1:T(8,128)(2,1)S(1)}, bf16[2048,64]{0,1:T(8,128)(2,1)}, u32[]{:S(2)}) %copy-start.2) | copy-done | bytes 262168
  4.8 0.0 copy-start.3
  4.8 0.9 %copy-done.3 = bf16[64,16,128]{2,1,0:T(8,128)(2,1)S(1)} copy-done((bf16[64,16,128]{2,1,0:T(8,128)(2,1)S(1)}, bf16[64,16,128]{2,1,0:T(8,128)(2,1)}, u32[]{:S(2)}) %copy-start.3) | copy-done | bytes 262168
  5.7 0.0 copy-start.4
  5.7 0.9 %copy-done.4 = bf16[64,16,128]{2,1,0:T(8,128)(2,1)S(1)} copy-done((bf16[64,16,128]{2,1,0:T(8,128)(2,1)S(1)}, bf16[64,16,128]{2,1,0:T(8,128)(2,1)}, u32[]{:S(2)}) %copy-start.4) | copy-done | bytes 262168
  6.7 0.0 copy-start.5
  6.7 0.9 %copy-done.5 = f32[136,128]{1,0:T(8,128)S(1)} copy-done((f32[136,128]{1,0:T(8,128)S(1)}, f32[136,128]{1,0:T(8,128)}, u32[]{:S(2)}) %copy-start.5) | copy-done | bytes 69656
  7.6 0.0 copy-start.6
  7.6 0.7 %copy-done.6 = f32[32,128]{1,0:T(8,128)S(1)} copy-done((f32[32,128]{1,0:T(8,128)S(1)}, f32[32,128]{1,0:T(8,128)}, u32[]{:S(2)}) %copy-start.6) | copy-done | bytes 16408
  8.3 0.0 copy-start.7
  8.3 0.7 %copy-done.7 = f32[2048]{0:T(1024)S(1)} copy-done((f32[2048]{0:T(1024)S(1)}, f32[2048]{0:T(1024)}, u32[]{:S(2)}) %copy-start.7) | copy-done | bytes 8216
  9.0 0.0 copy-start.8
  9.0 0.7 %copy-done.8 = f32[512]{0:T(512)S(1)} copy-done((f32[512]{0:T(512)S(1)}, f32[512]{0:T(512)}, u32[]{:S(2)}) %copy-start.8) | copy-done | bytes 2072
  9.6 0.0 copy-start.9
  9.7 0.7 %copy-done.9 = bf16[1,2,128]{2,1,0:T(2,128)(2,1)S(1)} copy-done((bf16[1,2,128]{2,1,0:T(2,128)(2,1)S(1)}, bf16[1,2,128]{2,1,0:T(2,128)(2,1)}, u32[]{:S(2)}) %copy-start.9) | copy-done | bytes 536
  10.3 0.0 copy-start.10
  10.3 0.7 %copy-done.10 = bf16[1,2,64]{2,1,0:T(2,128)(2,1)S(1)} copy-done((bf16[1,2,64]{2,1,0:T(2,128)(2,1)S(1)}, bf16[1,2,64]{2,1,0:T(2,128)(2,1)}, u32[]{:S(2)}) %copy-start.10) | copy-done | bytes 280
  11.0 33.1 %shard_map.130 = (bf16[64,4096]{1,0:T(8,128)(2,1)S(1)}, bf16[8,4096]{1,0:T(8,128)(2,1)S(1)}, bf16[2,128]{1,0:T(2,128)(2,1)S(1)}) custom-call(bf16[16,32,2048]{2,1,0:T(8,128)(2,1)S(1)} %copy-done, f32[1,2048]{1,0:T(1,128)S(1)} %bitcast.19, bf16[2048,512]{1,0:T(8,128)(2,1)S(1)} %copy-done.1, bf16[64,2048]{1,0:T(8,128)(2,1)S(1)} %bitcast.15, ...), custom_call_target="tpu_custom_call" | custom-call | tf_op jit(solution)/shard_map/pallas_call | solution.py:356
  44.1 0.8 %copy.17 = bf16[1,4096,64]{1,2,0:T(8,128)(2,1)} copy(bf16[1,4096,64]{1,2,0:T(8,128)(2,1)S(1)} %bitcast.14) | data formatting | bytes 1048576
  44.9 0.6 %copy.18 = bf16[1,4096,8]{1,2,0:T(8,128)(2,1)} copy(bf16[1,4096,8]{1,2,0:T(8,128)(2,1)S(1)} %bitcast.18) | data formatting | bytes 131072
  45.5 0.5 %copy.19 = bf16[1,2,128]{2,1,0:T(2,128)(2,1)} copy(bf16[1,2,128]{2,1,0:T(2,128)(2,1)S(1)} %bitcast.23) | data formatting | bytes 1024
Async XLA Ops:
  0.6 1.6 %copy-start = (bf16[16,32,2048]{2,1,0:T(8,128)(2,1)S(1)}, bf16[16,32,2048]{2,1,0:T(8,128)(2,1)}, u32[]{:S(2)}) copy-start(bf16[16,32,2048]{2,1,0:T(8,128)(2,1)} %x_hbm.1) | copy-start | bytes 6291460
  2.2 1.6 %copy-start.1 = (bf16[2048,512]{1,0:T(8,128)(2,1)S(1)}, bf16[2048,512]{1,0:T(8,128)(2,1)}, u32[]{:S(2)}) copy-start(bf16[2048,512]{1,0:T(8,128)(2,1)} %w_hbm.1) | copy-start | bytes 6291460
  3.8 0.9 %copy-start.2 = (bf16[2048,64]{0,1:T(8,128)(2,1)S(1)}, bf16[2048,64]{0,1:T(8,128)(2,1)}, u32[]{:S(2)}) copy-start(bf16[2048,64]{0,1:T(8,128)(2,1)} %param.14) | copy-start | bytes 786436
  4.8 0.9 %copy-start.3 = (bf16[64,16,128]{2,1,0:T(8,128)(2,1)S(1)}, bf16[64,16,128]{2,1,0:T(8,128)(2,1)}, u32[]{:S(2)}) copy-start(bf16[64,16,128]{2,1,0:T(8,128)(2,1)} %param.16) | copy-start | bytes 786436
  5.7 0.9 %copy-start.4 = (bf16[64,16,128]{2,1,0:T(8,128)(2,1)S(1)}, bf16[64,16,128]{2,1,0:T(8,128)(2,1)}, u32[]{:S(2)}) copy-start(bf16[64,16,128]{2,1,0:T(8,128)(2,1)} %param.17) | copy-start | bytes 786436
  6.7 0.9 %copy-start.5 = (f32[136,128]{1,0:T(8,128)S(1)}, f32[136,128]{1,0:T(8,128)}, u32[]{:S(2)}) copy-start(f32[136,128]{1,0:T(8,128)} %constant.4.clone.tab_hbm) | copy-start | bytes 208900
  7.6 0.7 %copy-start.6 = (f32[32,128]{1,0:T(8,128)S(1)}, f32[32,128]{1,0:T(8,128)}, u32[]{:S(2)}) copy-start(f32[32,128]{1,0:T(8,128)} %constant.5.clone.off_hbm) | copy-start | bytes 49156
  8.3 0.7 %copy-start.7 = (f32[2048]{0:T(1024)S(1)}, f32[2048]{0:T(1024)}, u32[]{:S(2)}) copy-start(f32[2048]{0:T(1024)} %param.12) | copy-start | bytes 24580
  9.0 0.7 %copy-start.8 = (f32[512]{0:T(512)S(1)}, f32[512]{0:T(512)}, u32[]{:S(2)}) copy-start(f32[512]{0:T(512)} %param.15) | copy-start | bytes 6148
  9.6 0.7 %copy-start.9 = (bf16[1,2,128]{2,1,0:T(2,128)(2,1)S(1)}, bf16[1,2,128]{2,1,0:T(2,128)(2,1)}, u32[]{:S(2)}) copy-start(bf16[1,2,128]{2,1,0:T(2,128)(2,1)} %param.18) | copy-start | bytes 1540
  10.3 0.7 %copy-start.10 = (bf16[1,2,64]{2,1,0:T(2,128)(2,1)S(1)}, bf16[1,2,64]{2,1,0:T(2,128)(2,1)}, u32[]{:S(2)}) copy-start(bf16[1,2,64]{2,1,0:T(2,128)(2,1)} %param.19) | copy-start | bytes 772

commit v2 on v1

--- a/solution.py
+++ b/solution.py
@@ -39,11 +39,10 @@
 
 def kernel(
     x_hbm, gain_hbm, w_hbm, rd_hbm, scal_hbm, look_hbm, pay_hbm, qn_hbm, qr_hbm, tab_hbm, off_hbm,
-    out_s, out_r, out_f,
+    krecv, rrecv, read_out,
     xb, gain, w, rd, scal, look, pay, tab, off,
-    kst, kall, qn, qr, aall, pst, pall, ktst, rtst, krecv, rrecv, asc, arecv, sbuf,
-    ostage, rstage, fstage,
-    lsem, wsem, ksend, krsem, qsend, qrsem, asend, arsem, psend, prsem, k2send, k2rsem, csend, crsem, osem,
+    kst, kall, qn, qr, aall, pst, pall, ktst, rtst, asc, arecv, sbuf,
+    lsem, wsem, ksend, krsem, qsend, qrsem, asend, arsem, psend, prsem, k2send, k2rsem, csend, crsem,
 ):
     sp, tp = lax.axis_index("sp"), lax.axis_index("tp")
     z, y = sp // 4, lax.rem(sp, 4)
@@ -291,25 +290,35 @@
     second = jnp.dot(mixed, pall[1], preferred_element_type=F32)
     values = jnp.where(iota((16, 128), 0) == 0, first, second)[:2]
     values = values * lax.rsqrt(jnp.mean(values * values, axis=1, keepdims=True) + EPS)
-    fstage[...] = values.astype(BF16)
-    pltpu.make_async_copy(fstage, out_f, osem.at[8]).start()
-
-    def out_copies(g):
-        lanes = pl.ds(pl.multiple_of(g * 1024, 1024), 1024)
-        return (
-            pltpu.make_async_copy(ostage.at[g], out_s.at[:, lanes], osem.at[g]),
-            pltpu.make_async_copy(rstage.at[g], out_r.at[:, lanes], osem.at[4 + g]),
-        )
-
-    def finish(k, _):
-        g = group_of(k)
-
-        def wait(step, _):
+    read_out[...] = values.astype(BF16)
+
+    def wait_k2(step, _):
+        for g in range(4):
             for c in k2_copies(step, g, tp_of(8 - step)):
                 c.wait_recv()
-            return 0
-
-        lax.fori_loop(1, 8, wait, 0)
+        return 0
+
+    lax.fori_loop(1, 8, wait_k2, 0)
+
+    def drain(step, _):
+        for c in q_copies(step, tp) + (a_copy(step, tp), p_copy(step, tp), c_copy(step, tp)):
+            c.wait_send()
+        for g in range(4):
+            for c in k2_copies(step, g, tp):
+                c.wait_send()
+        return 0
+
+    lax.fori_loop(1, 8, drain, 0)
+    for n in range(16):
+        if n != 12:
+            k_copy(n, (n // 4 + 1) % 4, n % 4, my_slot).wait_send()
+
+
+def arrange(krecv, rrecv, read_in, out_s, out_r, out_f, ostage, rstage, sem):
+    read = pltpu.make_async_copy(read_in, out_f, sem.at[8])
+    read.start()
+    copies = [read]
+    for g in range(4):
         for source, stage, rows in ((krecv, ostage, 64), (rrecv, rstage, 8)):
             lane = jnp.right_shift(iota((rows, 128), 1), 5)
             for u in range(2):
@@ -323,45 +332,31 @@
                         v = pltpu.roll(v, 128 - 32 * a, 1)
                     at = 256 * a + 128 * u
                     stage[g, :, at : at + 128] = v.astype(BF16)
-        for c in out_copies(g):
+        lanes = pl.ds(1024 * g, 1024)
+        copies.append(pltpu.make_async_copy(ostage.at[g], out_s.at[:, lanes], sem.at[g]))
+        copies.append(pltpu.make_async_copy(rstage.at[g], out_r.at[:, lanes], sem.at[4 + g]))
+        for c in copies[-2:]:
             c.start()
-        return 0
-
-    lax.fori_loop(0, 4, finish, 0)
-
-    def drain(step, _):
-        for c in q_copies(step, tp) + (a_copy(step, tp), p_copy(step, tp), c_copy(step, tp)):
-            c.wait_send()
-        for g in range(4):
-            for c in k2_copies(step, g, tp):
-                c.wait_send()
-        return 0
-
-    lax.fori_loop(1, 8, drain, 0)
-    for n in range(16):
-        if n != 12:
-            k_copy(n, (n // 4 + 1) % 4, n % 4, my_slot).wait_send()
-    for g in range(4):
-        for c in out_copies(g):
-            c.wait()
-    pltpu.make_async_copy(fstage, out_f, osem.at[8]).wait()
+    for c in copies:
+        c.wait()
 
 
 def solution(mesh):
     first, offset = trig_tables(128, 32, 64)
 
     def step(x, gain, w, rd, scal, look, payload, qn, qr):
-        any_space = pl.BlockSpec(memory_space=pl.ANY)
+        hbm = pl.BlockSpec(memory_space=pltpu.HBM)
+        vmem = pl.BlockSpec(memory_space=pltpu.VMEM)
         dma = pltpu.SemaphoreType.DMA
-        stored, rotary, read = pl.pallas_call(
+        received = pl.pallas_call(
             kernel,
             out_shape=(
-                jax.ShapeDtypeStruct((64, 4096), BF16),
-                jax.ShapeDtypeStruct((8, 4096), BF16),
+                jax.ShapeDtypeStruct((4, 8, 64, 128), BF16),
+                jax.ShapeDtypeStruct((4, 8, 8, 128), BF16),
                 jax.ShapeDtypeStruct((2, 128), BF16),
             ),
-            in_specs=[any_space] * 11,
-            out_specs=(any_space,) * 3,
+            in_specs=[hbm] * 11,
+            out_specs=(vmem,) * 3,
             scratch_shapes=[
                 pltpu.VMEM((16, 32, 2048), BF16),
                 pltpu.VMEM((1, 2048), F32),
@@ -381,14 +376,9 @@
                 pltpu.VMEM((2, 512, 128), BF16),
                 pltpu.VMEM((4, 8, 64, 128), BF16),
                 pltpu.VMEM((4, 8, 8, 128), BF16),
-                pltpu.VMEM((4, 8, 64, 128), BF16),
-                pltpu.VMEM((4, 8, 8, 128), BF16),
                 pltpu.VMEM((8, 2, 640), F32),
                 pltpu.VMEM((8, 2, 640), F32),
                 pltpu.VMEM((4, 16, 128), F32),
-                pltpu.VMEM((4, 64, 1024), BF16),
-                pltpu.VMEM((4, 8, 1024), BF16),
-                pltpu.VMEM((2, 128), BF16),
                 dma((16,)),
                 dma((10,)),
                 dma((16,)),
@@ -403,15 +393,35 @@
                 dma((2, 4, 8)),
                 dma((8,)),
                 dma((8,)),
-                dma((9,)),
             ],
             compiler_params=pltpu.CompilerParams(
                 collective_id=0, has_side_effects=True, vmem_limit_bytes=48 * 1024 * 1024
             ),
         )(
-            x, gain.reshape(1, 2048), w, rd.T, scal.reshape(1, 512), look.reshape(1024, 128),
-            payload.reshape(1024, 128), qn.reshape(2, 128), qr.reshape(2, 64), jnp.asarray(first), jnp.asarray(offset),
-        )
+            *(
+                pltpu.with_memory_space_constraint(v, pltpu.HBM)
+                for v in (
+                    x, gain.reshape(1, 2048), w, rd.T, scal.reshape(1, 512), look.reshape(1024, 128),
+                    payload.reshape(1024, 128), qn.reshape(2, 128), qr.reshape(2, 64),
+                    jnp.asarray(first), jnp.asarray(offset),
+                )
+            )
+        )
+        stored, rotary, read = pl.pallas_call(
+            arrange,
+            out_shape=(
+                jax.ShapeDtypeStruct((64, 4096), BF16),
+                jax.ShapeDtypeStruct((8, 4096), BF16),
+                jax.ShapeDtypeStruct((2, 128), BF16),
+            ),
+            in_specs=[vmem] * 3,
+            out_specs=(hbm,) * 3,
+            scratch_shapes=[
+                pltpu.VMEM((4, 64, 1024), BF16),
+                pltpu.VMEM((4, 8, 1024), BF16),
+                dma((9,)),
+            ],
+        )(*(pltpu.with_memory_space_constraint(v, pltpu.VMEM) for v in received))
         return stored.T[None], rotary.T[None], read[None]
 
     tp = "tp"

time: 46.5 us -> 31.1 us (0.67)
  local copies, waits for them, and re-layouts: 12.2 us -> 0 us
  Pallas kernels: 33.1 us -> 30.4 us
    unnamed x25 -> x0, local copies, waits for them, and re-layouts: 12.2 us -> none
    pallas_call x1 -> x2, Pallas kernels: 33.1 us -> 30.4 us  [the longest x1 29.3 us: step(): pl.pallas_call(kernel, out_shape=(jax.ShapeDtypeStruct((4, 8, 64, 128), B...]
where the time goes in v2:
time: 31.1 us; the launch traced here: 31 us
  Pallas kernels  30.4 us (98%)
  between operations  0.64 us (2%)
    pallas_call x1, Pallas kernels, step(): pl.pallas_call(kernel, out_shape=(jax.ShapeDtypeStruct((4, 8, 64, 128), B...  29.3 us
    pallas_call x1, Pallas kernels, step(): pl.pallas_call(arrange, out_shape=(jax.ShapeDtypeStruct((64, 4096), BF16)...  1.04 us

profile of v2, /device:TPU:1, one launch (start us, length us, event | category | flops | bytes accessed | tf_op | source)
XLA Modules:
  0.0 31.0 jit_solution(12737384972363549038)
XLA Ops:
  0.6 29.3 %shard_map.130 = (bf16[4,8,64,128]{3,2,1,0:T(8,128)(2,1)S(1)}, bf16[4,8,8,128]{3,2,1,0:T(8,128)(2,1)S(1)}, bf16[2,128]{1,0:T(2,128)(2,1)S(1)}) custom-call(bf16[16,32,2048]{2,1,0:T(8,128)(2,1)} %x_hbm.1, f32[1,2048]{1,0:T(1,128)} %bitcast.17, bf16[2048,512]{1,0:T(8,128)(2,1)} %w_hbm.1, bf16[64,2048]{1,0:T(8,128)(2,1)} %bitcast.14, f32[1,512]{1,0:T(1,128)} %bitcast.18, ...), custom_call_target="tpu_custom_call" | custom-call | tf_op jit(solution)/shard_map/pallas_call | solution.py:351
  30.0 1.0 %shard_map.131 = (bf16[64,4096]{1,0:T(8,128)(2,1)}, bf16[8,4096]{1,0:T(8,128)(2,1)}, bf16[2,128]{1,0:T(2,128)(2,1)}) custom-call(bf16[4,8,64,128]{3,2,1,0:T(8,128)(2,1)S(1)} %get-tuple-element.9.krecv, bf16[4,8,8,128]{3,2,1,0:T(8,128)(2,1)S(1)} %get-tuple-element.10.rrecv, bf16[2,128]{1,0:T(2,128)(2,1)S(1)} %get-tuple-element.11.read_in), custom_call_target="tpu_custom_call" | custom-call | tf_op jit(solution)/shard_map/pallas_call | solution.py:410

commit v3 on v2

v3 whole, which is shorter than its diff:
```python
import jax
import jax.numpy as jnp
import numpy as np
from jax import lax
from jax.experimental import pallas as pl
from jax.experimental.pallas import tpu as pltpu
from jax.sharding import PartitionSpec as P

MESH = pl.DeviceIdType.MESH
EPS = 1e-6
ROPE_BASE = 10000.0
F32 = jnp.float32
BF16 = jnp.bfloat16

NT = (((1,), (1,)), ((), ()))

STEPS = (
    (2, 2), (1, 2), (3, 2), (2, 1),
    (2, 3), (1, 1), (3, 3), (1, 3),
    (3, 1), (2, 0), (0, 2), (1, 0),
    (3, 0), (0, 1), (0, 3), (0, 0),
)


def trig_tables(blocks, rows, rope):
    half = rope // 2
    freq = 1.0 / ROPE_BASE ** (np.arange(half, dtype=np.float64) * 2.0 / rope)
    freq = np.concatenate([freq, freq])
    first = np.arange(blocks + 8, dtype=np.float64)[:, None] * rows * freq
    offset = np.arange(rows, dtype=np.float64)[:, None] * freq

    def both(angle):
        return np.concatenate([np.cos(angle), np.sin(angle)], axis=1).astype(np.float32)

    return both(first), both(offset)


def half_swap(v):
    half = v.shape[-1] // 2
    return jnp.concatenate([v[..., half:], v[..., :half]], axis=-1)


def iota(shape, dim):
    return lax.broadcasted_iota(jnp.int32, shape, dim)


def sp_at(sp, dz, dy):
    return lax.rem(sp // 4 + dz, 4) * 4 + lax.rem(lax.rem(sp, 4) + dy, 4)


def kernel(
    x_hbm, gain_hbm, w_hbm, rd_hbm, scal_hbm, look_hbm, pay_hbm, qn_hbm, qr_hbm, tab_hbm, off_hbm,
    krecv, rrecv, read_out,
    xb, gain, w, rd, scal, look, pay, tab, off,
    kst, rst, kall, rall, qn, qr, aall, pst, pall, ktst, rtst, asc, arecv,
    xsem, wsem, ksend, krsem, rsend, rrsem, qsend, qrsem, small, k2sem,
):
    sp, tp = lax.axis_index("sp"), lax.axis_index("tp")

    def tp_of(step):
        return lax.rem(tp + step, 8)

    for n in range(4):
        pltpu.make_async_copy(x_hbm.at[sp_at(sp, *STEPS[n])], xb.at[n], xsem.at[0]).start()
    halves = [pl.ds(0, 1024), pl.ds(1024, 1024)]
    loads = [
        pltpu.make_async_copy(src, dst, wsem.at[n])
        for n, (src, dst) in enumerate(
            (
                (gain_hbm, gain), (w_hbm.at[halves[0]], w.at[halves[0]]), (w_hbm.at[halves[1]], w.at[halves[1]]),
                (rd_hbm, rd), (scal_hbm, scal), (tab_hbm, tab), (off_hbm, off),
                (look_hbm, look), (pay_hbm, pay), (qn_hbm, qn.at[tp]), (qr_hbm, qr.at[tp]),
            )
        )
    ]
    for c in loads[:7]:
        c.start()

    barrier = pltpu.get_barrier_semaphore()

    def greet_sp(n, _):
        pl.semaphore_signal(barrier, inc=1, device_id=(lax.rem(sp + n, 16), tp), device_id_type=MESH)
        return 0

    def greet_tp(n, _):
        pl.semaphore_signal(barrier, inc=1, device_id=(sp, tp_of(n)), device_id_type=MESH)
        return 0

    lax.fori_loop(1, 16, greet_sp, 0)
    lax.fori_loop(1, 8, greet_tp, 0)

    def to_tp(src, dst, send, recv, step):
        return pltpu.make_async_remote_copy(
            src_ref=src, dst_ref=dst, send_sem=send, recv_sem=recv,
            device_id=(sp, tp_of(step)), device_id_type=MESH,
        )

    def to_all_tp(copies):
        def send(step, _):
            for c in copies(step):
                c.start()
            return 0

        lax.fori_loop(1, 8, send, 0)

    def to_sp(src, dst, send, recv, n):
        return pltpu.make_async_remote_copy(
            src_ref=src, dst_ref=dst, send_sem=send, recv_sem=recv,
            device_id=(sp_at(sp, *STEPS[n]), tp), device_id_type=MESH,
        )

    for c in loads[5:7]:
        c.wait()
    sign = jnp.where(iota((32, 64), 1) < 32, -1.0, 1.0).astype(F32)
    base = tab[pl.ds(sp * 8 + tp, 1), :]
    offs = off[...]
    cos = base[:, :64] * offs[:, :64] - base[:, 64:] * offs[:, 64:]
    sin = (base[:, 64:] * offs[:, :64] + base[:, :64] * offs[:, 64:]) * sign
    cos4 = jnp.concatenate([cos] * 4, axis=0)
    sin4 = jnp.concatenate([sin] * 4, axis=0)
    loads[0].wait()

    def project(k):
        pltpu.make_async_copy(x_hbm.at[pl.ds(0, 4)], xb.at[pl.ds(4 * k, 4)], xsem.at[k]).wait()
        xv = xb[4 * k : 4 * k + 4].reshape(128, 2048).astype(F32)
        scale = lax.rsqrt(jnp.mean(xv * xv, axis=1, keepdims=True) + EPS)
        normed = (xv * scale * gain[...]).astype(BF16)
        if k == 0:
            loads[1].wait()
        latent = jnp.dot(normed[:, :1024], w[:1024], preferred_element_type=F32)
        if k == 0:
            for c in loads[2:5]:
                c.wait()
            for n in range(4, 16):
                pltpu.make_async_copy(x_hbm.at[sp_at(sp, *STEPS[n])], xb.at[n], xsem.at[n // 4]).start()
            for c in loads[7:]:
                c.start()
        latent += jnp.dot(normed[:, 1024:], w[1024:], preferred_element_type=F32)
        latent = latent.astype(BF16).astype(F32)
        rot = lax.dot_general(normed, rd[...], NT, preferred_element_type=F32).astype(BF16).astype(F32)
        scale = lax.rsqrt(jnp.mean(latent * latent, axis=1, keepdims=True) + EPS)
        stored = (latent * scale * scal[...]).astype(BF16).reshape(4, 32, 512)
        turned = (rot * cos4 + half_swap(rot) * sin4).reshape(4, 2, 16, 64)
        turned = jnp.concatenate([turned[:, 0], turned[:, 1]], axis=-1).astype(BF16)
        kst[4 * k : 4 * k + 4] = stored
        rst[4 * k : 4 * k + 4] = turned
        if k == 3:
            kall[12 + lax.rem(3 + tp, 4)] = stored[3]
            rall[12 + lax.rem(3 + tp, 4)] = turned[3]
        if k == 0:
            pl.semaphore_wait(barrier, 22)
        for n in range(4 * k, min(4 * k + 4, 15)):
            slot = 4 * k + lax.rem(n + tp, 4)
            to_sp(kst.at[n], kall.at[slot], ksend, krsem.at[k], n).start()
            to_sp(rst.at[n], rall.at[slot], rsend, rrsem.at[k], n).start()

    def arrived(k):
        count = 4 if k < 3 else 3
        at = pl.ds(4 * k, count)
        to_sp(kst.at[at], kall.at[at], ksend, krsem.at[k], 0).wait_recv()
        to_sp(rst.at[at], rall.at[at], rsend, rrsem.at[k], 0).wait_recv()

    project(0)
    to_all_tp(
        lambda step: (
            to_tp(qn_hbm, qn.at[tp], qsend.at[0], qrsem.at[0], step),
            to_tp(qr_hbm, qr.at[tp], qsend.at[1], qrsem.at[1], step),
        )
    )

    loads[8].wait()
    row, col = iota((256, 256), 0), iota((256, 256), 1)
    wanted = jnp.bitwise_and(row, 15) * 16 + jnp.right_shift(row, 4)
    order = jnp.where(col == wanted, 1.0, 0.0).astype(BF16)
    for g in range(4):
        rows = jnp.dot(order, pay[256 * g : 256 * (g + 1), :], preferred_element_type=F32)
        pst[:, :, 16 * g : 16 * (g + 1), :] = rows.astype(BF16).reshape(8, 2, 16, 128)
    mine = pl.ds(pl.multiple_of(tp * 64, 64), 64)
    pall[:, mine, :] = pst[tp]
    to_all_tp(lambda step: (to_tp(pst.at[tp_of(step)], pall.at[:, mine, :], small.at[0], small.at[1], step),))

    project(1)
    project(2)

    for n in (7, 9, 10):
        loads[n].wait()
    seven = pl.ds(0, 7)
    to_tp(qn.at[seven], qn.at[seven], qsend.at[0], qrsem.at[0], 1).wait_recv()
    to_tp(qr.at[seven], qr.at[seven], qsend.at[1], qrsem.at[1], 1).wait_recv()
    q_all = qn[...].astype(F32).reshape(16, 128).astype(BF16)
    t_all = qr[...].astype(F32).reshape(16, 64)
    parts = lax.dot_general(q_all, look[...], NT, preferred_element_type=F32)
    same = jnp.bitwise_and(iota((16, 1024), 1), 15) == iota((16, 1024), 0)
    parts = jnp.where(same, parts, 0.0).astype(BF16)
    pick = jnp.right_shift(iota((1024, 128), 0), 4) + 64 * lax.rem(tp, 2) == iota((1024, 128), 1)
    pick = jnp.where(pick, 1.0, 0.0).astype(BF16)
    aall[tp] = jnp.dot(parts, pick, preferred_element_type=F32).astype(BF16)
    to_all_tp(lambda step: (to_tp(aall.at[tp], aall.at[tp], small.at[2], small.at[3], step),))
    last = tab[128:129, :]
    q_turn = (t_all * last[:, :64] + half_swap(t_all) * (last[:, 64:] * sign[:1])).astype(BF16)

    project(3)

    def keys(k):
        packed = rall[4 * k : 4 * k + 4].astype(F32)
        swapped = half_swap(packed)
        rows = jnp.concatenate([packed[:, None, :, :64], swapped[:, None, :, :64]], axis=1)
        return rows.reshape(128, 64)

    def spread(k, rows):
        ktst[k] = kall[4 * k : 4 * k + 4].reshape(128, 512).T.reshape(8, 64, 128)
        rtst[k] = rows.T.reshape(8, 8, 128).astype(BF16)
        to_all_tp(
            lambda step: (
                to_tp(ktst.at[k, tp_of(step)], krecv.at[k, tp], k2sem.at[0], k2sem.at[1], step),
                to_tp(rtst.at[k, tp_of(step)], rrecv.at[k, tp], k2sem.at[2], k2sem.at[3], step),
            )
        )
        krecv[k, tp] = ktst[k, tp]
        rrecv[k, tp] = rtst[k, tp]

    rows = []
    for k in range(3):
        arrived(k)
        rows.append(keys(k))
        spread(k, rows[k])

    to_tp(aall.at[seven], aall.at[seven], small.at[2], small.at[3], 1).wait_recv()
    absorbed = jnp.concatenate([aall[2 * u] + aall[2 * u + 1] for u in range(4)], axis=1)

    def scores(k, rows):
        latent = kall[4 * k : 4 * k + 4].reshape(128, 512)
        total = lax.dot_general(absorbed, latent, NT, preferred_element_type=F32)
        total += lax.dot_general(q_turn, rows.astype(BF16), NT, preferred_element_type=F32)
        return total * (192.0 ** -0.5)

    def mixed(weight, k):
        latent = kall[4 * k : 4 * k + 4].reshape(128, 512)
        return jnp.dot(weight.astype(BF16), latent, preferred_element_type=F32)

    seen = [scores(k, rows[k]) for k in range(3)]
    top_seen = jnp.max(jnp.maximum(jnp.maximum(seen[0], seen[1]), seen[2]), axis=1, keepdims=True)
    weights = [jnp.exp(s - top_seen) for s in seen]
    total_seen = jnp.sum(weights[0] + weights[1] + weights[2], axis=1, keepdims=True)
    context_seen = mixed(weights[0], 0) + mixed(weights[1], 1) + mixed(weights[2], 2)

    arrived(3)
    last_rows = keys(3)
    late = scores(3, last_rows)
    top = jnp.maximum(top_seen, jnp.max(late, axis=1, keepdims=True))
    weight = jnp.exp(late - top)
    shrink = jnp.exp(top_seen - top)
    total = total_seen * shrink + jnp.sum(weight, axis=1, keepdims=True)
    context = context_seen * shrink + mixed(weight, 3)
    stats = jnp.where(iota((16, 128), 1) < 64, top, total)
    for t in range(8):
        asc[t, :, :512] = context[2 * t : 2 * t + 2]
        asc[t, :, 512:] = stats[2 * t : 2 * t + 2]
    to_all_tp(lambda step: (to_tp(asc.at[tp_of(step)], arecv.at[tp], small.at[4], small.at[5], step),))
    arecv[tp] = asc[tp]
    spread(3, last_rows)

    to_tp(pst.at[seven], pst.at[seven], small.at[0], small.at[1], 1).wait_recv()
    to_tp(asc.at[seven], arecv.at[seven], small.at[4], small.at[5], 1).wait_recv()
    got = arecv[...]
    tops, totals = got[:, :, 512:513], got[:, :, 576:577]
    share = jnp.exp(tops - jnp.max(tops, axis=0, keepdims=True))
    summed = jnp.sum(got[:, :, :512] * share, axis=0) / jnp.sum(totals * share, axis=0)
    summed = jnp.concatenate([summed, jnp.zeros((14, 512), F32)], axis=0).astype(BF16)
    first = jnp.dot(summed, pall[0], preferred_element_type=F32)
    second = jnp.dot(summed, pall[1], preferred_element_type=F32)
    values = jnp.where(iota((16, 128), 0) == 0, first, second)[:2]
    values = values * lax.rsqrt(jnp.mean(values * values, axis=1, keepdims=True) + EPS)
    read_out[...] = values.astype(BF16)

    sent = pl.ds(0, 15)
    to_sp(kst.at[sent], kall.at[sent], ksend, krsem.at[0], 0).wait_send()
    to_sp(rst.at[sent], rall.at[sent], rsend, rrsem.at[0], 0).wait_send()
    to_tp(qn.at[seven], qn.at[seven], qsend.at[0], qrsem.at[0], 1).wait_send()
    to_tp(qr.at[seven], qr.at[seven], qsend.at[1], qrsem.at[1], 1).wait_send()
    to_tp(pst.at[seven], pst.at[seven], small.at[0], small.at[1], 1).wait_send()
    to_tp(aall.at[seven], aall.at[seven], small.at[2], small.at[3], 1).wait_send()
    to_tp(asc.at[seven], arecv.at[seven], small.at[4], small.at[5], 1).wait_send()
    blocks = to_tp(ktst.at[:, seven], krecv.at[:, seven], k2sem.at[0], k2sem.at[1], 1)
    turned = to_tp(rtst.at[:, seven], rrecv.at[:, seven], k2sem.at[2], k2sem.at[3], 1)
    for c in (blocks, turned):
        c.wait_send()
        c.wait_recv()


def arrange(krecv, rrecv, read_in, out_s, out_r, out_f, stage, turned_stage, sem):
    sp = lax.axis_index("sp")
    read = pltpu.make_async_copy(read_in, out_f, sem.at[2])
    read.start()
    for k in range(4):
        at = [256 * sp_at(sp, (4 - dz) % 4, (4 - dy) % 4) for dz, dy in STEPS[4 * k : 4 * k + 4]]
        for source, held, rows in ((krecv, stage, 64), (rrecv, turned_stage, 8)):
            lane = jnp.right_shift(iota((rows, 128), 1), 5)
            for u in range(2):
                blocks = [source[k, 4 * u + j].astype(F32) for j in range(4)]
                for a in range(4):
                    mine = [jnp.bitwise_and(lane - a, 3) == j for j in range(3)]
                    v = jnp.where(
                        mine[0], blocks[0], jnp.where(mine[1], blocks[1], jnp.where(mine[2], blocks[2], blocks[3]))
                    )
                    if a:
                        v = pltpu.roll(v, 128 - 32 * a, 1)
                    held[:, pl.ds(pl.multiple_of(at[a] + 128 * u, 128), 128)] = v.astype(BF16)
        for a in range(4):
            lanes = pl.ds(pl.multiple_of(at[a], 256), 256)
            pltpu.make_async_copy(stage.at[:, lanes], out_s.at[:, lanes], sem.at[0]).start()
    turned = pltpu.make_async_copy(turned_stage, out_r, sem.at[1])
    turned.start()
    pltpu.make_async_copy(stage, out_s, sem.at[0]).wait()
    turned.wait()
    read.wait()


def solution(mesh):
    first, offset = trig_tables(128, 32, 64)

    def step(x, gain, w, rd, scal, look, payload, qn, qr):
        hbm = pl.BlockSpec(memory_space=pltpu.HBM)
        vmem = pl.BlockSpec(memory_space=pltpu.VMEM)
        dma = pltpu.SemaphoreType.DMA
        received = pl.pallas_call(
            kernel,
            out_shape=(
                jax.ShapeDtypeStruct((4, 8, 64, 128), BF16),
                jax.ShapeDtypeStruct((4, 8, 8, 128), BF16),
                jax.ShapeDtypeStruct((2, 128), BF16),
            ),
            in_specs=[hbm] * 11,
            out_specs=(vmem,) * 3,
            scratch_shapes=[
                pltpu.VMEM((16, 32, 2048), BF16),
                pltpu.VMEM((1, 2048), F32),
                pltpu.VMEM((2048, 512), BF16),
                pltpu.VMEM((64, 2048), BF16),
                pltpu.VMEM((1, 512), F32),
                pltpu.VMEM((1024, 128), BF16),
                pltpu.VMEM((1024, 128), BF16),
                pltpu.VMEM((136, 128), F32),
                pltpu.VMEM((32, 128), F32),
                pltpu.VMEM((16, 32, 512), BF16),
                pltpu.VMEM((16, 16, 128), BF16),
                pltpu.VMEM((16, 32, 512), BF16),
                pltpu.VMEM((16, 16, 128), BF16),
                pltpu.VMEM((8, 2, 128), BF16),
                pltpu.VMEM((8, 2, 64), BF16),
                pltpu.VMEM((8, 16, 128), BF16),
                pltpu.VMEM((8, 2, 64, 128), BF16),
                pltpu.VMEM((2, 512, 128), BF16),
                pltpu.VMEM((4, 8, 64, 128), BF16),
                pltpu.VMEM((4, 8, 8, 128), BF16),
                pltpu.VMEM((8, 2, 640), F32),
                pltpu.VMEM((8, 2, 640), F32),
                dma((4,)),
                dma((11,)),
                dma,
                dma((4,)),
                dma,
                dma((4,)),
                dma((2,)),
                dma((2,)),
                dma((6,)),
                dma((4,)),
            ],
            compiler_params=pltpu.CompilerParams(
                collective_id=0, has_side_effects=True, vmem_limit_bytes=48 * 1024 * 1024
            ),
        )(
            *(
                pltpu.with_memory_space_constraint(v, pltpu.HBM)
                for v in (
                    x, gain.reshape(1, 2048), w, rd.T, scal.reshape(1, 512), look.reshape(1024, 128),
                    payload.reshape(1024, 128), qn.reshape(2, 128), qr.reshape(2, 64),
                    jnp.asarray(first), jnp.asarray(offset),
                )
            )
        )
        stored, rotary, read = pl.pallas_call(
            arrange,
            out_shape=(
                jax.ShapeDtypeStruct((64, 4096), BF16),
                jax.ShapeDtypeStruct((8, 4096), BF16),
                jax.ShapeDtypeStruct((2, 128), BF16),
            ),
            in_specs=[vmem] * 3,
            out_specs=(hbm,) * 3,
            scratch_shapes=[
                pltpu.VMEM((64, 4096), BF16),
                pltpu.VMEM((8, 4096), BF16),
                dma((3,)),
            ],
        )(*(pltpu.with_memory_space_constraint(v, pltpu.VMEM) for v in received))
        return stored.T[None], rotary.T[None], read[None]

    tp = "tp"
    both = ("sp", "tp")
    in_specs = (
        P(None, both, None), P(), P(), P(), P(), P(tp, None, None), P(tp, None, None),
        P("sp", tp, None), P("sp", tp, None),
    )
    out_specs = (P("sp", None, tp), P("sp", None, tp), P("sp", tp, None))
    return jax.shard_map(step, mesh=mesh, in_specs=in_specs, out_specs=out_specs, check_vma=False)
```

time: 31.1 us -> 29.2 us (0.939)
  Pallas kernels: 30.4 us -> 28.4 us
    pallas_call x1, Pallas kernels: 29.3 us -> 27.4 us  [step(): pl.pallas_call(kernel, out_shape=(jax.ShapeDtypeStruct((4, 8, 64, 128), B...]
where the time goes in v3:
time: 29.2 us; the launch traced here: 29.1 us
  Pallas kernels  28.4 us (97%)
  between operations  0.64 us (2%)
    pallas_call x1, Pallas kernels, step(): pl.pallas_call(kernel, out_shape=(jax.ShapeDtypeStruct((4, 8, 64, 128), B...  27.4 us
    pallas_call x1, Pallas kernels, step(): pl.pallas_call(arrange, out_shape=(jax.ShapeDtypeStruct((64, 4096), BF16)...  0.99 us

profile of v3, /device:TPU:1, one launch (start us, length us, event | category | flops | bytes accessed | tf_op | source)
XLA Modules:
  0.0 29.1 jit_solution(2328535563084862256)
XLA Ops:
  0.6 27.4 %shard_map.130 = (bf16[4,8,64,128]{3,2,1,0:T(8,128)(2,1)S(1)}, bf16[4,8,8,128]{3,2,1,0:T(8,128)(2,1)S(1)}, bf16[2,128]{1,0:T(2,128)(2,1)S(1)}) custom-call(bf16[16,32,2048]{2,1,0:T(8,128)(2,1)} %x_hbm.1, f32[1,2048]{1,0:T(1,128)} %bitcast.17, bf16[2048,512]{1,0:T(8,128)(2,1)} %w_hbm.1, bf16[64,2048]{1,0:T(8,128)(2,1)} %bitcast.14, f32[1,512]{1,0:T(1,128)} %bitcast.18, ...), custom_call_target="tpu_custom_call" | custom-call | tf_op jit(solution)/shard_map/pallas_call | solution.py:326
  28.1 1.0 %shard_map.131 = (bf16[64,4096]{1,0:T(8,128)(2,1)}, bf16[8,4096]{1,0:T(8,128)(2,1)}, bf16[2,128]{1,0:T(2,128)(2,1)}) custom-call(bf16[4,8,64,128]{3,2,1,0:T(8,128)(2,1)S(1)} %get-tuple-element.9.krecv, bf16[4,8,8,128]{3,2,1,0:T(8,128)(2,1)S(1)} %get-tuple-element.10.rrecv, bf16[2,128]{1,0:T(2,128)(2,1)S(1)} %get-tuple-element.11.read_in), custom_call_target="tpu_custom_call" | custom-call | tf_op jit(solution)/shard_map/pallas_call | solution.py:382

commit v4 on v3

--- a/solution.py
+++ b/solution.py
@@ -15,11 +15,13 @@
 NT = (((1,), (1,)), ((), ()))
 
 STEPS = (
-    (2, 2), (1, 2), (3, 2), (2, 1),
-    (2, 3), (1, 1), (3, 3), (1, 3),
-    (3, 1), (2, 0), (0, 2), (1, 0),
-    (3, 0), (0, 1), (0, 3), (0, 0),
+    (1, 1), (3, 3), (2, 0), (0, 2),
+    (1, 3), (3, 1), (1, 2), (3, 2),
+    (2, 1), (2, 3), (1, 0), (3, 0),
+    (0, 1), (0, 3), (2, 2), (0, 0),
 )
+OWN = STEPS.index((0, 0))
+OTHERS = 1 if OWN == 0 else 0
 
 
 def trig_tables(blocks, rows, rope):
@@ -52,7 +54,7 @@
     x_hbm, gain_hbm, w_hbm, rd_hbm, scal_hbm, look_hbm, pay_hbm, qn_hbm, qr_hbm, tab_hbm, off_hbm,
     krecv, rrecv, read_out,
     xb, gain, w, rd, scal, look, pay, tab, off,
-    kst, rst, kall, rall, qn, qr, aall, pst, pall, ktst, rtst, asc, arecv,
+    kst, rst, kall, rall, qn, qr, aall, pst, pall, ktst, rtst, asc, arecv, order, part, held,
     xsem, wsem, ksend, krsem, rsend, rrsem, qsend, qrsem, small, k2sem,
 ):
     sp, tp = lax.axis_index("sp"), lax.axis_index("tp")
@@ -60,34 +62,32 @@
     def tp_of(step):
         return lax.rem(tp + step, 8)
 
-    for n in range(4):
-        pltpu.make_async_copy(x_hbm.at[sp_at(sp, *STEPS[n])], xb.at[n], xsem.at[0]).start()
     halves = [pl.ds(0, 1024), pl.ds(1024, 1024)]
     loads = [
         pltpu.make_async_copy(src, dst, wsem.at[n])
         for n, (src, dst) in enumerate(
             (
-                (gain_hbm, gain), (w_hbm.at[halves[0]], w.at[halves[0]]), (w_hbm.at[halves[1]], w.at[halves[1]]),
+                (gain_hbm, gain), (w_hbm.at[halves[0]], w.at[halves[0], pl.ds(0, 512)]),
+                (w_hbm.at[halves[1]], w.at[halves[1], pl.ds(0, 512)]),
                 (rd_hbm, rd), (scal_hbm, scal), (tab_hbm, tab), (off_hbm, off),
                 (look_hbm, look), (pay_hbm, pay), (qn_hbm, qn.at[tp]), (qr_hbm, qr.at[tp]),
             )
         )
     ]
-    for c in loads[:7]:
-        c.start()
+    for n in (5, 6, 0, 3):
+        loads[n].start()
+    for n in range(4):
+        pltpu.make_async_copy(x_hbm.at[sp_at(sp, *STEPS[n])], xb.at[n], xsem.at[0]).start()
+    loads[1].start()
 
     barrier = pltpu.get_barrier_semaphore()
-
-    def greet_sp(n, _):
-        pl.semaphore_signal(barrier, inc=1, device_id=(lax.rem(sp + n, 16), tp), device_id_type=MESH)
-        return 0
-
-    def greet_tp(n, _):
-        pl.semaphore_signal(barrier, inc=1, device_id=(sp, tp_of(n)), device_id_type=MESH)
-        return 0
-
-    lax.fori_loop(1, 16, greet_sp, 0)
-    lax.fori_loop(1, 8, greet_tp, 0)
+    for dz, dy in sorted(STEPS, key=lambda s: -min(s[0], 4 - s[0]) - min(s[1], 4 - s[1]))[:15]:
+        pl.semaphore_signal(barrier, inc=1, device_id=(sp_at(sp, dz, dy), tp), device_id_type=MESH)
+    for step in (4, 5, 3, 2, 6, 7, 1):
+        pl.semaphore_signal(barrier, inc=1, device_id=(sp, tp_of(step)), device_id_type=MESH)
+
+    for n in (4, 2):
+        loads[n].start()
 
     def to_tp(src, dst, send, recv, step):
         return pltpu.make_async_remote_copy(
@@ -116,51 +116,73 @@
     offs = off[...]
     cos = base[:, :64] * offs[:, :64] - base[:, 64:] * offs[:, 64:]
     sin = (base[:, 64:] * offs[:, :64] + base[:, :64] * offs[:, 64:]) * sign
-    cos4 = jnp.concatenate([cos] * 4, axis=0)
-    sin4 = jnp.concatenate([sin] * 4, axis=0)
     loads[0].wait()
 
-    def project(k):
-        pltpu.make_async_copy(x_hbm.at[pl.ds(0, 4)], xb.at[pl.ds(4 * k, 4)], xsem.at[k]).wait()
-        xv = xb[4 * k : 4 * k + 4].reshape(128, 2048).astype(F32)
+    row, col = iota((256, 256), 0), iota((256, 256), 1)
+    wanted = jnp.bitwise_and(row, 15) * 16 + jnp.right_shift(row, 4)
+    order[...] = jnp.where(col == wanted, 1.0, 0.0).astype(BF16)
+    loads[3].wait()
+    w[:, 512:] = jnp.concatenate([rd[...].T, jnp.zeros((2048, 64), BF16)], axis=1)
+
+    def project(k, groups):
+        count = 4 * groups
+        for n in range(groups):
+            at = pl.ds(4 * (k + n), 4)
+            pltpu.make_async_copy(x_hbm.at[pl.ds(0, 4)], xb.at[at], xsem.at[k + n]).wait()
+        xv = xb[4 * k : 4 * k + count].reshape(32 * count, 2048).astype(F32)
         scale = lax.rsqrt(jnp.mean(xv * xv, axis=1, keepdims=True) + EPS)
         normed = (xv * scale * gain[...]).astype(BF16)
         if k == 0:
+            rot = jnp.dot(normed, w[:, 512:], preferred_element_type=F32)
+        else:
+            both = jnp.dot(normed, w[...], preferred_element_type=F32)
+            latent, rot = both[:, :512], both[:, 512:]
+        rot = rot[:, :64].astype(BF16).astype(F32)
+        turn = [jnp.concatenate([part] * count, axis=0) for part in (cos, sin)]
+        turned = (rot * turn[0] + half_swap(rot) * turn[1]).reshape(count, 2, 16, 64)
+        turned = jnp.concatenate([turned[:, 0], turned[:, 1]], axis=-1).astype(BF16)
+        rst[4 * k : 4 * k + count] = turned
+        if k == 0:
             loads[1].wait()
-        latent = jnp.dot(normed[:, :1024], w[:1024], preferred_element_type=F32)
-        if k == 0:
-            for c in loads[2:5]:
-                c.wait()
-            for n in range(4, 16):
+            for n in range(4, 8):
                 pltpu.make_async_copy(x_hbm.at[sp_at(sp, *STEPS[n])], xb.at[n], xsem.at[n // 4]).start()
-            for c in loads[7:]:
-                c.start()
-        latent += jnp.dot(normed[:, 1024:], w[1024:], preferred_element_type=F32)
+            part[...] = jnp.dot(normed[:, :1024], w[:1024, :512], preferred_element_type=F32)
+            held[...] = normed
+
+            @pl.when(sp >= 0)
+            def _():
+                for n in (2, 4):
+                    loads[n].wait()
+                for n in (8, 9, 10, 7):
+                    loads[n].start()
+                for n in range(8, 16):
+                    pltpu.make_async_copy(x_hbm.at[sp_at(sp, *STEPS[n])], xb.at[n], xsem.at[n // 4]).start()
+
+            normed = held[...]
+            latent = part[...] + jnp.dot(normed[:, 1024:], w[1024:, :512], preferred_element_type=F32)
         latent = latent.astype(BF16).astype(F32)
-        rot = lax.dot_general(normed, rd[...], NT, preferred_element_type=F32).astype(BF16).astype(F32)
         scale = lax.rsqrt(jnp.mean(latent * latent, axis=1, keepdims=True) + EPS)
-        stored = (latent * scale * scal[...]).astype(BF16).reshape(4, 32, 512)
-        turned = (rot * cos4 + half_swap(rot) * sin4).reshape(4, 2, 16, 64)
-        turned = jnp.concatenate([turned[:, 0], turned[:, 1]], axis=-1).astype(BF16)
-        kst[4 * k : 4 * k + 4] = stored
-        rst[4 * k : 4 * k + 4] = turned
-        if k == 3:
-            kall[12 + lax.rem(3 + tp, 4)] = stored[3]
-            rall[12 + lax.rem(3 + tp, 4)] = turned[3]
+        stored = (latent * scale * scal[...]).astype(BF16).reshape(count, 32, 512)
+        kst[4 * k : 4 * k + count] = stored
+        if 4 * k <= OWN < 4 * k + count:
+            slot = OWN // 4 * 4 + lax.rem(OWN + tp, 4)
+            kall[slot] = stored[OWN - 4 * k]
+            rall[slot] = rst[OWN]
         if k == 0:
             pl.semaphore_wait(barrier, 22)
-        for n in range(4 * k, min(4 * k + 4, 15)):
-            slot = 4 * k + lax.rem(n + tp, 4)
-            to_sp(kst.at[n], kall.at[slot], ksend, krsem.at[k], n).start()
-            to_sp(rst.at[n], rall.at[slot], rsend, rrsem.at[k], n).start()
+        for n in range(4 * k, 4 * k + count):
+            if n != OWN:
+                slot = n // 4 * 4 + lax.rem(n + tp, 4)
+                to_sp(kst.at[n], kall.at[slot], ksend, krsem.at[n // 4], n).start()
+                to_sp(rst.at[n], rall.at[slot], rsend, rrsem.at[n // 4], n).start()
 
     def arrived(k):
-        count = 4 if k < 3 else 3
+        count = 4 if k != OWN // 4 else 3
         at = pl.ds(4 * k, count)
-        to_sp(kst.at[at], kall.at[at], ksend, krsem.at[k], 0).wait_recv()
-        to_sp(rst.at[at], rall.at[at], rsend, rrsem.at[k], 0).wait_recv()
-
-    project(0)
+        to_sp(kst.at[at], kall.at[at], ksend, krsem.at[k], OTHERS).wait_recv()
+        to_sp(rst.at[at], rall.at[at], rsend, rrsem.at[k], OTHERS).wait_recv()
+
+    project(0, 1)
     to_all_tp(
         lambda step: (
             to_tp(qn_hbm, qn.at[tp], qsend.at[0], qrsem.at[0], step),
@@ -168,19 +190,18 @@
         )
     )
 
+    project(1, 1)
+
     loads[8].wait()
-    row, col = iota((256, 256), 0), iota((256, 256), 1)
-    wanted = jnp.bitwise_and(row, 15) * 16 + jnp.right_shift(row, 4)
-    order = jnp.where(col == wanted, 1.0, 0.0).astype(BF16)
     for g in range(4):
-        rows = jnp.dot(order, pay[256 * g : 256 * (g + 1), :], preferred_element_type=F32)
+        rows = jnp.dot(order[...], pay[256 * g : 256 * (g + 1), :], preferred_element_type=F32)
         pst[:, :, 16 * g : 16 * (g + 1), :] = rows.astype(BF16).reshape(8, 2, 16, 128)
     mine = pl.ds(pl.multiple_of(tp * 64, 64), 64)
     pall[:, mine, :] = pst[tp]
     to_all_tp(lambda step: (to_tp(pst.at[tp_of(step)], pall.at[:, mine, :], small.at[0], small.at[1], step),))
 
-    project(1)
-    project(2)
+    project(2, 1)
+    project(3, 1)
 
     for n in (7, 9, 10):
         loads[n].wait()
@@ -199,8 +220,6 @@
     last = tab[128:129, :]
     q_turn = (t_all * last[:, :64] + half_swap(t_all) * (last[:, 64:] * sign[:1])).astype(BF16)
 
-    project(3)
-
     def keys(k):
         packed = rall[4 * k : 4 * k + 4].astype(F32)
         swapped = half_swap(packed)
@@ -273,9 +292,9 @@
     values = values * lax.rsqrt(jnp.mean(values * values, axis=1, keepdims=True) + EPS)
     read_out[...] = values.astype(BF16)
 
-    sent = pl.ds(0, 15)
-    to_sp(kst.at[sent], kall.at[sent], ksend, krsem.at[0], 0).wait_send()
-    to_sp(rst.at[sent], rall.at[sent], rsend, rrsem.at[0], 0).wait_send()
+    sent = pl.ds(OTHERS, 15)
+    to_sp(kst.at[sent], kall.at[sent], ksend, krsem.at[0], OTHERS).wait_send()
+    to_sp(rst.at[sent], rall.at[sent], rsend, rrsem.at[0], OTHERS).wait_send()
     to_tp(qn.at[seven], qn.at[seven], qsend.at[0], qrsem.at[0], 1).wait_send()
     to_tp(qr.at[seven], qr.at[seven], qsend.at[1], qrsem.at[1], 1).wait_send()
     to_tp(pst.at[seven], pst.at[seven], small.at[0], small.at[1], 1).wait_send()
@@ -335,7 +354,7 @@
             scratch_shapes=[
                 pltpu.VMEM((16, 32, 2048), BF16),
                 pltpu.VMEM((1, 2048), F32),
-                pltpu.VMEM((2048, 512), BF16),
+                pltpu.VMEM((2048, 640), BF16),
                 pltpu.VMEM((64, 2048), BF16),
                 pltpu.VMEM((1, 512), F32),
                 pltpu.VMEM((1024, 128), BF16),
@@ -355,6 +374,9 @@
                 pltpu.VMEM((4, 8, 8, 128), BF16),
                 pltpu.VMEM((8, 2, 640), F32),
                 pltpu.VMEM((8, 2, 640), F32),
+                pltpu.VMEM((256, 256), BF16),
+                pltpu.VMEM((128, 512), F32),
+                pltpu.VMEM((128, 2048), BF16),
                 dma((4,)),
                 dma((11,)),
                 dma,

time: 29.2 us -> 25.7 us (0.88)
  Pallas kernels: 28.4 us -> 25 us
    pallas_call x1, Pallas kernels: 27.4 us -> 24 us  [step(): pl.pallas_call(kernel, out_shape=(jax.ShapeDtypeStruct((4, 8, 64, 128), B...]
where the time goes in v4:
time: 25.7 us; the launch traced here: 25.6 us
  Pallas kernels  25 us (97%)
  between operations  0.64 us (2%)
    pallas_call x1, Pallas kernels, step(): pl.pallas_call(kernel, out_shape=(jax.ShapeDtypeStruct((4, 8, 64, 128), B...  24 us
    pallas_call x1, Pallas kernels, step(): pl.pallas_call(arrange, out_shape=(jax.ShapeDtypeStruct((64, 4096), BF16)...  0.99 us

profile of v4, /device:TPU:1, one launch (start us, length us, event | category | flops | bytes accessed | tf_op | source)
XLA Modules:
  0.0 25.6 jit_solution(2734601840781187782)
XLA Ops:
  0.6 24.0 %shard_map.130 = (bf16[4,8,64,128]{3,2,1,0:T(8,128)(2,1)S(1)}, bf16[4,8,8,128]{3,2,1,0:T(8,128)(2,1)S(1)}, bf16[2,128]{1,0:T(2,128)(2,1)S(1)}) custom-call(bf16[16,32,2048]{2,1,0:T(8,128)(2,1)} %x_hbm.1, f32[1,2048]{1,0:T(1,128)} %bitcast.17, bf16[2048,512]{1,0:T(8,128)(2,1)} %w_hbm.1, bf16[64,2048]{1,0:T(8,128)(2,1)} %bitcast.14, f32[1,512]{1,0:T(1,128)} %bitcast.18, ...), custom_call_target="tpu_custom_call" | custom-call | tf_op jit(solution)/shard_map/pallas_call | solution.py:345
  24.6 1.0 %shard_map.131 = (bf16[64,4096]{1,0:T(8,128)(2,1)}, bf16[8,4096]{1,0:T(8,128)(2,1)}, bf16[2,128]{1,0:T(2,128)(2,1)}) custom-call(bf16[4,8,64,128]{3,2,1,0:T(8,128)(2,1)S(1)} %get-tuple-element.9.krecv, bf16[4,8,8,128]{3,2,1,0:T(8,128)(2,1)S(1)} %get-tuple-element.10.rrecv, bf16[2,128]{1,0:T(2,128)(2,1)S(1)} %get-tuple-element.11.read_in), custom_call_target="tpu_custom_call" | custom-call | tf_op jit(solution)/shard_map/pallas_call | solution.py:404

commit v5 on v4

v5 whole, which is shorter than its diff:
```python
import jax
import jax.numpy as jnp
import numpy as np
from jax import lax
from jax.experimental import pallas as pl
from jax.experimental.pallas import tpu as pltpu
from jax.sharding import PartitionSpec as P

MESH = pl.DeviceIdType.MESH
EPS = 1e-6
ROPE_BASE = 10000.0
F32 = jnp.float32
BF16 = jnp.bfloat16

NT = (((1,), (1,)), ((), ()))

STEPS = (
    (1, 1), (3, 3), (2, 0), (0, 2),
    (1, 3), (3, 1), (1, 2), (3, 2),
    (2, 1), (2, 3), (1, 0), (3, 0),
    (0, 1), (0, 3), (2, 2), (0, 0),
)
OWN = STEPS.index((0, 0))
OTHERS = 1 if OWN == 0 else 0


def trig_tables(blocks, rows, rope):
    half = rope // 2
    freq = 1.0 / ROPE_BASE ** (np.arange(half, dtype=np.float64) * 2.0 / rope)
    freq = np.concatenate([freq, freq])
    first = np.arange(blocks + 8, dtype=np.float64)[:, None] * rows * freq
    offset = np.arange(rows, dtype=np.float64)[:, None] * freq

    def both(angle):
        return np.concatenate([np.cos(angle), np.sin(angle)], axis=1).astype(np.float32)

    return np.concatenate([both(first), both(offset)], axis=0)


def half_swap(v):
    half = v.shape[-1] // 2
    return jnp.concatenate([v[..., half:], v[..., :half]], axis=-1)


def iota(shape, dim):
    return lax.broadcasted_iota(jnp.int32, shape, dim)


def sp_at(sp, dz, dy):
    return lax.rem(sp // 4 + dz, 4) * 4 + lax.rem(lax.rem(sp, 4) + dy, 4)


def lanes_of(sp, n):
    dz, dy = STEPS[n]
    return pl.ds(pl.multiple_of(256 * sp_at(sp, (4 - dz) % 4, (4 - dy) % 4), 256), 256)


def arranged(source):
    blocks = [source[t].astype(F32) for t in range(8)]
    lane = jnp.right_shift(iota((72, 128), 1), 5)
    for a in range(4):
        mine = [jnp.bitwise_and(lane - a, 3) == j for j in range(3)]
        halves = []
        for u in range(2):
            b = blocks[4 * u : 4 * u + 4]
            v = jnp.where(mine[0], b[0], jnp.where(mine[1], b[1], jnp.where(mine[2], b[2], b[3])))
            halves.append(pltpu.roll(v, 128 - 32 * a, 1) if a else v)
        both = jnp.concatenate(halves, axis=1)
        yield a, both[:64].astype(BF16), both[64:].astype(BF16)


def kernel(
    x_hbm, gain_hbm, w_hbm, rd_hbm, scal_hbm, look_hbm, pay_hbm, qn_hbm, qr_hbm, tab_hbm,
    stage, turned_stage, read_out,
    xb, gain, w, rd, scal, look, pay, tab,
    kst, kall, qn, qr, aall, pst, pall, ktst, krecv, asc, arecv, part, held,
    xsem, wsem, krsem, qrsem, small, k2rsem,
):
    sp, tp = lax.axis_index("sp"), lax.axis_index("tp")

    def tp_of(step):
        return lax.rem(tp + step, 8)

    ksend, k2send, psend, asend, csend = (wsem.at[n] for n in (1, 2, 4, 5, 6))
    qsend = (wsem.at[3], wsem.at[7])

    barrier = pltpu.get_barrier_semaphore()
    steps = sorted(STEPS, key=lambda s: -min(s[0], 4 - s[0]) - min(s[1], 4 - s[1]))[:15]

    def greet(some):
        for dz, dy in some:
            pl.semaphore_signal(barrier, inc=1, device_id=(sp_at(sp, dz, dy), tp), device_id_type=MESH)

    greet(steps[:5])

    halves = [pl.ds(0, 1024), pl.ds(1024, 1024)]
    loads = [
        pltpu.make_async_copy(src, dst, wsem.at[n % 9])
        for n, (src, dst) in enumerate(
            (
                (gain_hbm, gain), (w_hbm.at[halves[0]], w.at[halves[0], pl.ds(0, 512)]),
                (w_hbm.at[halves[1]], w.at[halves[1], pl.ds(0, 512)]),
                (rd_hbm, rd), (scal_hbm, scal), (tab_hbm, tab),
                (pay_hbm, pay), (qn_hbm, qn.at[tp]), (qr_hbm, qr.at[tp]), (look_hbm, look),
            )
        )
    ]
    for n in (6, 5, 0, 7, 8, 3):
        loads[n].start()
    for n in range(4):
        pltpu.make_async_copy(x_hbm.at[sp_at(sp, *STEPS[n])], xb.at[n], xsem.at[0]).start()
    loads[1].start()

    greet(steps[5:])
    for step in (4, 5, 3, 2, 6, 7, 1):
        pl.semaphore_signal(barrier, inc=1, device_id=(sp, tp_of(step)), device_id_type=MESH)
    for n in (4, 2):
        loads[n].start()

    def to_tp(src, dst, send, recv, step):
        return pltpu.make_async_remote_copy(
            src_ref=src, dst_ref=dst, send_sem=send, recv_sem=recv,
            device_id=(sp, tp_of(step)), device_id_type=MESH,
        )

    def to_all_tp(copies):
        for step in (4, 5, 3, 2, 6, 7, 1):
            for c in copies(step):
                c.start()

    def to_sp(src, dst, send, recv, n):
        return pltpu.make_async_remote_copy(
            src_ref=src, dst_ref=dst, send_sem=send, recv_sem=recv,
            device_id=(sp_at(sp, *STEPS[n]), tp), device_id_type=MESH,
        )

    row, col = iota((256, 256), 0), iota((256, 256), 1)
    wanted = jnp.bitwise_and(row, 15) * 16 + jnp.right_shift(row, 4)
    order = jnp.where(col == wanted, 1.0, 0.0).astype(BF16)
    loads[6].wait()
    for g in range(4):
        rows = jnp.dot(order, pay[256 * g : 256 * (g + 1), :], preferred_element_type=F32)
        rows = rows.astype(BF16).reshape(8, 2, 16, 128)
        for head in range(2):
            pst[:, 16 * g : 16 * (g + 1), 128 * head : 128 * (head + 1)] = rows[:, head]
    mine = pl.ds(pl.multiple_of(tp * 64, 64), 64)
    pall[mine, :] = pst[tp]

    loads[5].wait()
    sign = jnp.where(iota((32, 64), 1) < 32, -1.0, 1.0).astype(F32)
    base = tab[pl.ds(sp * 8 + tp, 1), :]
    offs = tab[136:]
    cos = base[:, :64] * offs[:, :64] - base[:, 64:] * offs[:, 64:]
    sin = (base[:, 64:] * offs[:, :64] + base[:, :64] * offs[:, 64:]) * sign
    loads[0].wait()

    loads[3].wait()
    w[:, 512:] = jnp.concatenate([rd[...].T, jnp.zeros((2048, 64), BF16)], axis=1)

    def project(k, groups):
        count = 4 * groups
        for n in range(groups):
            at = pl.ds(4 * (k + n), 4)
            pltpu.make_async_copy(x_hbm.at[pl.ds(0, 4)], xb.at[at], xsem.at[(k + n) % 2]).wait()
        if k == 1:
            for n in range(12, 16):
                pltpu.make_async_copy(x_hbm.at[sp_at(sp, *STEPS[n])], xb.at[n], xsem.at[n // 4 % 2]).start()
        xv = xb[4 * k : 4 * k + count].reshape(32 * count, 2048).astype(F32)
        scale = lax.rsqrt(jnp.mean(xv * xv, axis=1, keepdims=True) + EPS)
        normed = (xv * scale * gain[...]).astype(BF16)
        if k == 0:
            rot = jnp.dot(normed, w[:, 512:], preferred_element_type=F32)
        else:
            both = jnp.dot(normed, w[...], preferred_element_type=F32)
            latent, rot = both[:, :512], both[:, 512:]
        rot = rot[:, :64].astype(BF16).astype(F32)
        turn = [jnp.concatenate([part] * count, axis=0) for part in (cos, sin)]
        turned = (rot * turn[0] + half_swap(rot) * turn[1]).reshape(count, 2, 16, 64)
        turned = jnp.concatenate([turned[:, 0], turned[:, 1]], axis=-1).astype(BF16)
        kst[4 * k : 4 * k + count, 128:] = turned
        if k == 0:
            loads[1].wait()
            for n in range(4, 8):
                pltpu.make_async_copy(x_hbm.at[sp_at(sp, *STEPS[n])], xb.at[n], xsem.at[n // 4 % 2]).start()
            part[...] = jnp.dot(normed[:, :1024], w[:1024, :512], preferred_element_type=F32)
            held[...] = normed

            @pl.when(sp >= 0)
            def _():
                for n in (2, 4):
                    loads[n].wait()
                loads[9].start()
                for n in range(8, 12):
                    pltpu.make_async_copy(x_hbm.at[sp_at(sp, *STEPS[n])], xb.at[n], xsem.at[n // 4 % 2]).start()

            normed = held[...]
            latent = part[...] + jnp.dot(normed[:, 1024:], w[1024:, :512], preferred_element_type=F32)
        latent = latent.astype(BF16).astype(F32)
        scale = lax.rsqrt(jnp.mean(latent * latent, axis=1, keepdims=True) + EPS)
        stored = (latent * scale * scal[...]).astype(BF16).reshape(count, 32, 512)
        for b in range(4):
            kst[4 * k : 4 * k + count, 32 * b : 32 * b + 32] = stored[:, :, 128 * b : 128 * b + 128]
        if 4 * k <= OWN < 4 * k + count:
            slot = OWN // 4 * 4 + lax.rem(OWN + tp, 4)
            kall[slot] = kst[OWN]
        if k == 0:
            pl.semaphore_wait(barrier, 22)
        for n in range(4 * k, 4 * k + count):
            if n != OWN:
                slot = n // 4 * 4 + lax.rem(n + tp, 4)
                to_sp(kst.at[n], kall.at[slot], ksend, krsem.at[n // 4], n).start()

    def arrived(k):
        count = 4 if k != OWN // 4 else 3
        at = pl.ds(4 * k, count)
        to_sp(kst.at[at], kall.at[at], ksend, krsem.at[k], OTHERS).wait_recv()

    for n in (7, 8):
        loads[n].wait()
    project(0, 1)
    to_all_tp(
        lambda step: (
            to_tp(qn.at[tp], qn.at[tp], qsend[0], qrsem.at[0], step),
            to_tp(qr.at[tp], qr.at[tp], qsend[1], qrsem.at[1], step),
        )
    )
    to_all_tp(lambda step: (to_tp(pst.at[tp_of(step)], pall.at[mine, :], psend, small.at[0], step),))
    project(1, 1)

    project(2, 1)
    project(3, 1)

    loads[9].wait()
    seven = pl.ds(0, 7)
    to_tp(qn.at[seven], qn.at[seven], qsend[0], qrsem.at[0], 1).wait_recv()
    to_tp(qr.at[seven], qr.at[seven], qsend[1], qrsem.at[1], 1).wait_recv()
    q_all = qn[...].astype(F32).reshape(16, 128).astype(BF16)
    t_all = qr[...].astype(F32).reshape(16, 64)
    parts = lax.dot_general(q_all, look[...], NT, preferred_element_type=F32)
    same = jnp.bitwise_and(iota((16, 1024), 1), 15) == iota((16, 1024), 0)
    parts = jnp.where(same, parts, 0.0).astype(BF16)
    pick = jnp.right_shift(iota((1024, 128), 0), 4) + 64 * lax.rem(tp, 2) == iota((1024, 128), 1)
    pick = jnp.where(pick, 1.0, 0.0).astype(BF16)
    aall[tp] = jnp.dot(parts, pick, preferred_element_type=F32).astype(BF16)
    to_all_tp(lambda step: (to_tp(aall.at[tp], aall.at[tp], asend, small.at[1], step),))
    last = tab[128:129, :]
    q_turn = (t_all * last[:, :64] + half_swap(t_all) * (last[:, 64:] * sign[:1])).astype(BF16)

    def keys(k):
        packed = kall[4 * k : 4 * k + 4, 128:].astype(F32)
        swapped = half_swap(packed)
        rows = jnp.concatenate([packed[:, None, :, :64], swapped[:, None, :, :64]], axis=1)
        return rows.reshape(128, 64)

    def latents(k):
        return jnp.concatenate(
            [kall[4 * k : 4 * k + 4, 32 * b : 32 * b + 32].reshape(128, 128) for b in range(4)], axis=1
        )

    def turned_over(k):
        block, turned = latents(k).T, keys(k).T.astype(BF16)
        ktst[k, :, :64] = block.reshape(8, 64, 128)
        ktst[k, :, 64:] = turned.reshape(8, 8, 128)
        return block, turned

    def spread(k):
        to_all_tp(lambda step: (to_tp(ktst.at[k, tp_of(step)], krecv.at[k, tp], k2send, k2rsem.at[k], step),))
        krecv[k, tp] = ktst[k, tp]

    here = []
    for k in range(3):
        arrived(k)
        here.append(turned_over(k))
        spread(k)

    to_tp(aall.at[seven], aall.at[seven], asend, small.at[1], 1).wait_recv()
    absorbed = jnp.concatenate([aall[2 * u] + aall[2 * u + 1] for u in range(4)], axis=1)

    def scores(block, turned):
        total = jnp.dot(absorbed, block, preferred_element_type=F32)
        total += jnp.dot(q_turn, turned, preferred_element_type=F32)
        return total * (192.0 ** -0.5)

    def mixed(weight, k):
        return jnp.dot(weight.astype(BF16), latents(k), preferred_element_type=F32)

    seen = [scores(*group) for group in here]
    top_seen = jnp.max(jnp.maximum(jnp.maximum(seen[0], seen[1]), seen[2]), axis=1, keepdims=True)
    weights = [jnp.exp(s - top_seen) for s in seen]
    total_seen = jnp.sum(weights[0] + weights[1] + weights[2], axis=1, keepdims=True)
    context_seen = mixed(weights[0], 0) + mixed(weights[1], 1) + mixed(weights[2], 2)

    arrived(3)
    late = scores(*turned_over(3))
    top = jnp.maximum(top_seen, jnp.max(late, axis=1, keepdims=True))
    weight = jnp.exp(late - top)
    shrink = jnp.exp(top_seen - top)
    total = total_seen * shrink + jnp.sum(weight, axis=1, keepdims=True)
    context = context_seen * shrink + mixed(weight, 3)
    stats = jnp.where(iota((16, 128), 1) < 64, top, total)
    for t in range(8):
        asc[t, :, :512] = context[2 * t : 2 * t + 2]
        asc[t, :, 512:] = stats[2 * t : 2 * t + 2]
    to_all_tp(lambda step: (to_tp(asc.at[tp_of(step)], arecv.at[tp], csend, small.at[2], step),))
    arecv[tp] = asc[tp]
    spread(3)

    def arrange(k):
        to_tp(ktst.at[k, seven], krecv.at[k, seven], k2send, k2rsem.at[k], 1).wait_recv()
        for a, block, turned in arranged(krecv.at[k]):
            lanes = lanes_of(sp, 4 * k + a)
            stage[:, lanes] = block
            turned_stage[:, lanes] = turned

    for k in range(3):
        arrange(k)

    to_tp(pst.at[seven], pst.at[seven], psend, small.at[0], 1).wait_recv()
    to_tp(asc.at[seven], arecv.at[seven], csend, small.at[2], 1).wait_recv()
    got = arecv[...]
    tops, totals = got[:, :, 512:513], got[:, :, 576:577]
    share = jnp.exp(tops - jnp.max(tops, axis=0, keepdims=True))
    summed = jnp.sum(got[:, :, :512] * share, axis=0) / jnp.sum(totals * share, axis=0)
    summed = jnp.concatenate([summed, jnp.zeros((14, 512), F32)], axis=0).astype(BF16)
    values = jnp.dot(summed, pall[...], preferred_element_type=F32)
    values = jnp.where(iota((16, 128), 0) == 0, values[:, :128], values[:, 128:])[:2]
    values = values * lax.rsqrt(jnp.mean(values * values, axis=1, keepdims=True) + EPS)
    read_out[...] = values.astype(BF16)

    sent = pl.ds(OTHERS, 15)
    to_sp(kst.at[sent], kall.at[sent], ksend, krsem.at[0], OTHERS).wait_send()
    to_tp(qn.at[seven], qn.at[seven], qsend[0], qrsem.at[0], 1).wait_send()
    to_tp(qr.at[seven], qr.at[seven], qsend[1], qrsem.at[1], 1).wait_send()
    to_tp(pst.at[seven], pst.at[seven], psend, small.at[0], 1).wait_send()
    to_tp(aall.at[seven], aall.at[seven], asend, small.at[1], 1).wait_send()
    to_tp(asc.at[seven], arecv.at[seven], csend, small.at[2], 1).wait_send()
    to_tp(ktst.at[:, seven], ktst.at[:, seven], k2send, k2rsem.at[3], 1).wait_send()
    arrange(3)


def finish(stage, turned_stage, read_in, out_s, out_r, out_f, sem):
    pieces = 4
    for n in range(pieces):
        lanes = pl.ds(4096 // pieces * n, 4096 // pieces)
        pltpu.make_async_copy(stage.at[:, lanes], out_s.at[:, lanes], sem.at[0]).start()
    others = [
        pltpu.make_async_copy(turned_stage, out_r, sem.at[1]), pltpu.make_async_copy(read_in, out_f, sem.at[2])
    ]
    for c in others:
        c.start()
    pltpu.make_async_copy(stage, out_s, sem.at[0]).wait()
    for c in others:
        c.wait()


def solution(mesh):
    angles = trig_tables(128, 32, 64)

    def step(x, gain, w, rd, scal, look, payload, qn, qr):
        hbm = pl.BlockSpec(memory_space=pltpu.HBM)
        vmem = pl.BlockSpec(memory_space=pltpu.VMEM)
        dma = pltpu.SemaphoreType.DMA
        received = pl.pallas_call(
            kernel,
            out_shape=(
                jax.ShapeDtypeStruct((64, 4096), BF16),
                jax.ShapeDtypeStruct((8, 4096), BF16),
                jax.ShapeDtypeStruct((2, 128), BF16),
            ),
            in_specs=[hbm] * 10,
            out_specs=(vmem,) * 3,
            scratch_shapes=[
                pltpu.VMEM((16, 32, 2048), BF16),
                pltpu.VMEM((1, 2048), F32),
                pltpu.VMEM((2048, 640), BF16),
                pltpu.VMEM((64, 2048), BF16),
                pltpu.VMEM((1, 512), F32),
                pltpu.VMEM((1024, 128), BF16),
                pltpu.VMEM((1024, 128), BF16),
                pltpu.VMEM((168, 128), F32),
                pltpu.VMEM((16, 144, 128), BF16),
                pltpu.VMEM((16, 144, 128), BF16),
                pltpu.VMEM((8, 2, 128), BF16),
                pltpu.VMEM((8, 2, 64), BF16),
                pltpu.VMEM((8, 16, 128), BF16),
                pltpu.VMEM((8, 64, 256), BF16),
                pltpu.VMEM((512, 256), BF16),
                pltpu.VMEM((4, 8, 72, 128), BF16),
                pltpu.VMEM((4, 8, 72, 128), BF16),
                pltpu.VMEM((8, 2, 640), F32),
                pltpu.VMEM((8, 2, 640), F32),
                pltpu.VMEM((128, 512), F32),
                pltpu.VMEM((128, 2048), BF16),
                dma((2,)),
                dma((9,)),
                dma((4,)),
                dma((2,)),
                dma((3,)),
                dma((4,)),
            ],
            compiler_params=pltpu.CompilerParams(
                collective_id=0, has_side_effects=True, vmem_limit_bytes=48 * 1024 * 1024
            ),
        )(
            *(
                pltpu.with_memory_space_constraint(v, pltpu.HBM)
                for v in (
                    x, gain.reshape(1, 2048), w, rd.T, scal.reshape(1, 512), look.reshape(1024, 128),
                    payload.reshape(1024, 128), qn.reshape(2, 128), qr.reshape(2, 64),
                    jnp.asarray(angles),
                )
            )
        )
        stored, rotary, read = pl.pallas_call(
            finish,
            out_shape=(
                jax.ShapeDtypeStruct((64, 4096), BF16),
                jax.ShapeDtypeStruct((8, 4096), BF16),
                jax.ShapeDtypeStruct((2, 128), BF16),
            ),
            in_specs=[vmem] * 3,
            out_specs=(hbm,) * 3,
            scratch_shapes=[dma((3,))],
        )(*(pltpu.with_memory_space_constraint(v, pltpu.VMEM) for v in received))
        return stored.T[None], rotary.T[None], read[None]

    tp = "tp"
    both = ("sp", "tp")
    in_specs = (
        P(None, both, None), P(), P(), P(), P(), P(tp, None, None), P(tp, None, None),
        P("sp", tp, None), P("sp", tp, None),
    )
    out_specs = (P("sp", None, tp), P("sp", None, tp), P("sp", tp, None))
    return jax.shard_map(step, mesh=mesh, in_specs=in_specs, out_specs=out_specs, check_vma=False)
```

time: 25.7 us -> 25.6 us (level)
  no operation moved by 1% of the time
where the time goes in v5:
time: 25.6 us; the launch traced here: 25.4 us
  Pallas kernels  24.8 us (97%)
  between operations  0.64 us (2%)
    pallas_call x1, Pallas kernels, step(): pl.pallas_call(kernel, out_shape=(jax.ShapeDtypeStruct((64, 4096), BF16),...  24 us
    pallas_call x1, Pallas kernels, step(): pl.pallas_call(finish, out_shape=(jax.ShapeDtypeStruct((64, 4096), BF16),...  0.83 us

profile of v5, /device:TPU:1, one launch (start us, length us, event | category | flops | bytes accessed | tf_op | source)
XLA Modules:
  0.0 25.4 jit_solution(8823220691706355013)
XLA Ops:
  0.6 24.0 %shard_map.121 = (bf16[64,4096]{1,0:T(8,128)(2,1)S(1)}, bf16[8,4096]{1,0:T(8,128)(2,1)S(1)}, bf16[2,128]{1,0:T(2,128)(2,1)S(1)}) custom-call(bf16[16,32,2048]{2,1,0:T(8,128)(2,1)} %x_hbm.1, f32[1,2048]{1,0:T(1,128)} %bitcast.17, bf16[2048,512]{1,0:T(8,128)(2,1)} %w_hbm.1, bf16[64,2048]{1,0:T(8,128)(2,1)} %bitcast.14, f32[1,512]{1,0:T(1,128)} %bitcast.18, ...), custom_call_target="tpu_custom_call" | custom-call | tf_op jit(solution)/shard_map/pallas_call | solution.py:363
  24.6 0.8 %shard_map.122 = (bf16[64,4096]{1,0:T(8,128)(2,1)}, bf16[8,4096]{1,0:T(8,128)(2,1)}, bf16[2,128]{1,0:T(2,128)(2,1)}) custom-call(bf16[64,4096]{1,0:T(8,128)(2,1)S(1)} %get-tuple-element.9.stage, bf16[8,4096]{1,0:T(8,128)(2,1)S(1)} %get-tuple-element.10.turned_stage, bf16[2,128]{1,0:T(2,128)(2,1)S(1)} %get-tuple-element.11.read_in), custom_call_target="tpu_custom_call" | custom-call | tf_op jit(solution)/shard_map/pallas_call | solution.py:414

commit v6 on v5

--- a/solution.py
+++ b/solution.py
@@ -15,10 +15,10 @@
 NT = (((1,), (1,)), ((), ()))
 
 STEPS = (
-    (1, 1), (3, 3), (2, 0), (0, 2),
-    (1, 3), (3, 1), (1, 2), (3, 2),
+    (2, 0), (0, 2), (1, 1), (3, 3),
+    (1, 2), (3, 2), (1, 3), (3, 1),
     (2, 1), (2, 3), (1, 0), (3, 0),
-    (0, 1), (0, 3), (2, 2), (0, 0),
+    (2, 2), (0, 1), (0, 3), (0, 0),
 )
 OWN = STEPS.index((0, 0))
 OTHERS = 1 if OWN == 0 else 0

time: 25.6 us -> 25.4 us (level)
  no operation moved by 1% of the time
where the time goes in v6:
time: 25.4 us; the launch traced here: 25.3 us
  Pallas kernels  24.6 us (97%)
  between operations  0.64 us (3%)
    pallas_call x1, Pallas kernels, step(): pl.pallas_call(kernel, out_shape=(jax.ShapeDtypeStruct((64, 4096), BF16),...  23.8 us
    pallas_call x1, Pallas kernels, step(): pl.pallas_call(finish, out_shape=(jax.ShapeDtypeStruct((64, 4096), BF16),...  0.83 us

profile of v6, /device:TPU:1, one launch (start us, length us, event | category | flops | bytes accessed | tf_op | source)
XLA Modules:
  0.0 25.3 jit_solution(6969772253611704151)
XLA Ops:
  0.6 23.8 %shard_map.121 = (bf16[64,4096]{1,0:T(8,128)(2,1)S(1)}, bf16[8,4096]{1,0:T(8,128)(2,1)S(1)}, bf16[2,128]{1,0:T(2,128)(2,1)S(1)}) custom-call(bf16[16,32,2048]{2,1,0:T(8,128)(2,1)} %x_hbm.1, f32[1,2048]{1,0:T(1,128)} %bitcast.17, bf16[2048,512]{1,0:T(8,128)(2,1)} %w_hbm.1, bf16[64,2048]{1,0:T(8,128)(2,1)} %bitcast.14, f32[1,512]{1,0:T(1,128)} %bitcast.18, ...), custom_call_target="tpu_custom_call" | custom-call | tf_op jit(solution)/shard_map/pallas_call | solution.py:363
  24.4 0.8 %shard_map.122 = (bf16[64,4096]{1,0:T(8,128)(2,1)}, bf16[8,4096]{1,0:T(8,128)(2,1)}, bf16[2,128]{1,0:T(2,128)(2,1)}) custom-call(bf16[64,4096]{1,0:T(8,128)(2,1)S(1)} %get-tuple-element.9.stage, bf16[8,4096]{1,0:T(8,128)(2,1)S(1)} %get-tuple-element.10.turned_stage, bf16[2,128]{1,0:T(2,128)(2,1)S(1)} %get-tuple-element.11.read_in), custom_call_target="tpu_custom_call" | custom-call | tf_op jit(solution)/shard_map/pallas_call | solution.py:414

commit v7 on v6

--- a/solution.py
+++ b/solution.py
@@ -224,8 +224,8 @@
             to_tp(qr.at[tp], qr.at[tp], qsend[1], qrsem.at[1], step),
         )
     )
+    project(1, 1)
     to_all_tp(lambda step: (to_tp(pst.at[tp_of(step)], pall.at[mine, :], psend, small.at[0], step),))
-    project(1, 1)
 
     project(2, 1)
     project(3, 1)
@@ -284,14 +284,15 @@
     def mixed(weight, k):
         return jnp.dot(weight.astype(BF16), latents(k), preferred_element_type=F32)
 
+    arrived(3)
+    final = turned_over(3)
     seen = [scores(*group) for group in here]
     top_seen = jnp.max(jnp.maximum(jnp.maximum(seen[0], seen[1]), seen[2]), axis=1, keepdims=True)
     weights = [jnp.exp(s - top_seen) for s in seen]
     total_seen = jnp.sum(weights[0] + weights[1] + weights[2], axis=1, keepdims=True)
     context_seen = mixed(weights[0], 0) + mixed(weights[1], 1) + mixed(weights[2], 2)
 
-    arrived(3)
-    late = scores(*turned_over(3))
+    late = scores(*final)
     top = jnp.maximum(top_seen, jnp.max(late, axis=1, keepdims=True))
     weight = jnp.exp(late - top)
     shrink = jnp.exp(top_seen - top)

time: 25.4 us -> 25.4 us (level)
  no operation moved by 1% of the time
where the time goes in v7:
time: 25.4 us; the launch traced here: 25.2 us
  Pallas kernels  24.6 us (97%)
  between operations  0.64 us (3%)
    pallas_call x1, Pallas kernels, step(): pl.pallas_call(kernel, out_shape=(jax.ShapeDtypeStruct((64, 4096), BF16),...  23.8 us
    pallas_call x1, Pallas kernels, step(): pl.pallas_call(finish, out_shape=(jax.ShapeDtypeStruct((64, 4096), BF16),...  0.83 us

profile of v7, /device:TPU:1, one launch (start us, length us, event | category | flops | bytes accessed | tf_op | source)
XLA Modules:
  0.0 25.2 jit_solution(5403261965464087002)
XLA Ops:
  0.6 23.8 %shard_map.121 = (bf16[64,4096]{1,0:T(8,128)(2,1)S(1)}, bf16[8,4096]{1,0:T(8,128)(2,1)S(1)}, bf16[2,128]{1,0:T(2,128)(2,1)S(1)}) custom-call(bf16[16,32,2048]{2,1,0:T(8,128)(2,1)} %x_hbm.1, f32[1,2048]{1,0:T(1,128)} %bitcast.17, bf16[2048,512]{1,0:T(8,128)(2,1)} %w_hbm.1, bf16[64,2048]{1,0:T(8,128)(2,1)} %bitcast.14, f32[1,512]{1,0:T(1,128)} %bitcast.18, ...), custom_call_target="tpu_custom_call" | custom-call | tf_op jit(solution)/shard_map/pallas_call | solution.py:364
  24.4 0.8 %shard_map.122 = (bf16[64,4096]{1,0:T(8,128)(2,1)}, bf16[8,4096]{1,0:T(8,128)(2,1)}, bf16[2,128]{1,0:T(2,128)(2,1)}) custom-call(bf16[64,4096]{1,0:T(8,128)(2,1)S(1)} %get-tuple-element.9.stage, bf16[8,4096]{1,0:T(8,128)(2,1)S(1)} %get-tuple-element.10.turned_stage, bf16[2,128]{1,0:T(2,128)(2,1)S(1)} %get-tuple-element.11.read_in), custom_call_target="tpu_custom_call" | custom-call | tf_op jit(solution)/shard_map/pallas_call | solution.py:415

commit v8 on v6

--- a/solution.py
+++ b/solution.py
@@ -91,7 +91,6 @@
         for dz, dy in some:
             pl.semaphore_signal(barrier, inc=1, device_id=(sp_at(sp, dz, dy), tp), device_id_type=MESH)
 
-    greet(steps[:5])
 
     halves = [pl.ds(0, 1024), pl.ds(1024, 1024)]
     loads = [
@@ -111,7 +110,7 @@
         pltpu.make_async_copy(x_hbm.at[sp_at(sp, *STEPS[n])], xb.at[n], xsem.at[0]).start()
     loads[1].start()
 
-    greet(steps[5:])
+    greet(steps)
     for step in (4, 5, 3, 2, 6, 7, 1):
         pl.semaphore_signal(barrier, inc=1, device_id=(sp, tp_of(step)), device_id_type=MESH)
     for n in (4, 2):

time: 25.4 us -> 25.4 us (level)
  no operation moved by 1% of the time
where the time goes in v8:
time: 25.4 us; the launch traced here: 25.3 us
  Pallas kernels  24.6 us (97%)
  between operations  0.64 us (3%)
    pallas_call x1, Pallas kernels, step(): pl.pallas_call(kernel, out_shape=(jax.ShapeDtypeStruct((64, 4096), BF16),...  23.8 us
    pallas_call x1, Pallas kernels, step(): pl.pallas_call(finish, out_shape=(jax.ShapeDtypeStruct((64, 4096), BF16),...  0.83 us

profile of v8, /device:TPU:1, one launch (start us, length us, event | category | flops | bytes accessed | tf_op | source)
XLA Modules:
  0.0 25.3 jit_solution(5423008644511776872)
XLA Ops:
  0.6 23.8 %shard_map.121 = (bf16[64,4096]{1,0:T(8,128)(2,1)S(1)}, bf16[8,4096]{1,0:T(8,128)(2,1)S(1)}, bf16[2,128]{1,0:T(2,128)(2,1)S(1)}) custom-call(bf16[16,32,2048]{2,1,0:T(8,128)(2,1)} %x_hbm.1, f32[1,2048]{1,0:T(1,128)} %bitcast.17, bf16[2048,512]{1,0:T(8,128)(2,1)} %w_hbm.1, bf16[64,2048]{1,0:T(8,128)(2,1)} %bitcast.14, f32[1,512]{1,0:T(1,128)} %bitcast.18, ...), custom_call_target="tpu_custom_call" | custom-call | tf_op jit(solution)/shard_map/pallas_call | solution.py:362
  24.4 0.8 %shard_map.122 = (bf16[64,4096]{1,0:T(8,128)(2,1)}, bf16[8,4096]{1,0:T(8,128)(2,1)}, bf16[2,128]{1,0:T(2,128)(2,1)}) custom-call(bf16[64,4096]{1,0:T(8,128)(2,1)S(1)} %get-tuple-element.9.stage, bf16[8,4096]{1,0:T(8,128)(2,1)S(1)} %get-tuple-element.10.turned_stage, bf16[2,128]{1,0:T(2,128)(2,1)S(1)} %get-tuple-element.11.read_in), custom_call_target="tpu_custom_call" | custom-call | tf_op jit(solution)/shard_map/pallas_call | solution.py:413

commit v9 on v6

--- a/solution.py
+++ b/solution.py
@@ -124,7 +124,7 @@
         )
 
     def to_all_tp(copies):
-        for step in (4, 5, 3, 2, 6, 7, 1):
+        for step in (3, 5, 4, 6, 2, 7, 1):
             for c in copies(step):
                 c.start()
 

time: 25.4 us -> 25.3 us (level)
  no operation moved by 1% of the time
where the time goes in v9:
time: 25.3 us; the launch traced here: 25.2 us
  Pallas kernels  24.5 us (97%)
  between operations  0.64 us (3%)
    pallas_call x1, Pallas kernels, step(): pl.pallas_call(kernel, out_shape=(jax.ShapeDtypeStruct((64, 4096), BF16),...  23.7 us
    pallas_call x1, Pallas kernels, step(): pl.pallas_call(finish, out_shape=(jax.ShapeDtypeStruct((64, 4096), BF16),...  0.83 us

profile of v9, /device:TPU:1, one launch (start us, length us, event | category | flops | bytes accessed | tf_op | source)
XLA Modules:
  0.0 25.2 jit_solution(3795305495006389758)
XLA Ops:
  0.6 23.7 %shard_map.121 = (bf16[64,4096]{1,0:T(8,128)(2,1)S(1)}, bf16[8,4096]{1,0:T(8,128)(2,1)S(1)}, bf16[2,128]{1,0:T(2,128)(2,1)S(1)}) custom-call(bf16[16,32,2048]{2,1,0:T(8,128)(2,1)} %x_hbm.1, f32[1,2048]{1,0:T(1,128)} %bitcast.17, bf16[2048,512]{1,0:T(8,128)(2,1)} %w_hbm.1, bf16[64,2048]{1,0:T(8,128)(2,1)} %bitcast.14, f32[1,512]{1,0:T(1,128)} %bitcast.18, ...), custom_call_target="tpu_custom_call" | custom-call | tf_op jit(solution)/shard_map/pallas_call | solution.py:363
  24.3 0.8 %shard_map.122 = (bf16[64,4096]{1,0:T(8,128)(2,1)}, bf16[8,4096]{1,0:T(8,128)(2,1)}, bf16[2,128]{1,0:T(2,128)(2,1)}) custom-call(bf16[64,4096]{1,0:T(8,128)(2,1)S(1)} %get-tuple-element.9.stage, bf16[8,4096]{1,0:T(8,128)(2,1)S(1)} %get-tuple-element.10.turned_stage, bf16[2,128]{1,0:T(2,128)(2,1)S(1)} %get-tuple-element.11.read_in), custom_call_target="tpu_custom_call" | custom-call | tf_op jit(solution)/shard_map/pallas_call | solution.py:414
